TPU v7x, 32 devices: a whole 2x2x4 slice. The times are simulated.
32 devices in a mesh: sp: 4 (over x, core), dp: 8 (over z, y).
Axes of the slice: x: 2, y: 2, z: 4, core: 2. Of those that a mesh axis runs over, the one named last changes fastest.
Arguments:
- content_features_raw: bfloat16 [8, 512, 3072], P('dp', 'sp'), may hold values from -6 to 6
- memory_entering_matrix: bfloat16 [8, 512, 2048], P('dp', 'sp'), may hold values from -6 to 6
- memory_leaving_matrix: bfloat16 [8, 512, 2048], P('dp', 'sp'), may hold values from -6 to 6
- feature_switch_signal: bfloat16 [8, 512, 3072], P('dp', 'sp'), may hold values from -6 to 6
- ahead_increment_raw: float32 [8, 512, 48], P('dp', 'sp'), may hold values from -5 to 5
- reverse_increment_raw: float32 [8, 512, 48], P('dp', 'sp'), may hold values from -5 to 5
- additional_fading: float32 [8, 512, 48], P('dp', 'sp'), as said below
- content_filter_weights: bfloat16 [4, 3072], P(None, 'sp'), may hold values from -3 to 3
- entering_filter_weights: bfloat16 [4, 2048], P(None, 'sp'), may hold values from -3 to 3
- leaving_filter_weights: bfloat16 [4, 2048], P(None, 'sp'), may hold values from -3 to 3
- increment_offset_lanes: float32 [2, 48], P(None, 'sp'), may hold values from -0.5 to 0.5
- fading_speed_exponents: float32 [2, 48], P(None, 'sp'), as said below
- result_scaling_factor: bfloat16 [3072], replicated, may hold values from 0.099609375 to 1.8984375
Outputs:
- out: bfloat16 [8, 512, 3072], P('dp', 'sp')
Inputs may be any that keep to these rules, and one draw needn't show every extreme that they name: Each head's row has a rate exp(fading_speed_exponents) between 0.3 / 4096 and 0.05. `additional_fading`: zero at most positions; elsewhere between log(0.5) and log(0.8).
All inputs are finite; a program needn't handle non-finite values.
Results may differ from a plain program's by a relative error of at most 0.0051.
Values may be sent and summed in bfloat16 or wider, within the bound.
No kernel may reach another device: no remote copies, remote signals or barrier semaphores. Data moves between devices by JAX's collectives and lax.ppermute only.
A program may use at most 64 MiB of HBM per device.

v0:
```python
import jax
import jax.numpy as jnp
from jax import lax
from jax.experimental import pallas as pl
from jax.experimental.pallas import tpu as pltpu
from jax.sharding import PartitionSpec as P

HEAD_DIM = 64
STATE = 128
BLK = 128
HIGH = lax.Precision.HIGHEST
f32 = jnp.float32
bf16 = jnp.bfloat16
ALL = ("dp", "sp")
STEP_HEADS = 6
SLOT = 8
RF, RB, CF, CB, FF, FB, EF, EB = range(8)


def iota(shape, dim):
    return lax.broadcasted_iota(jnp.int32, shape, dim)


def rates_kernel(ahead, back, fade, params, cols, rows, totals):
    steps = cols.shape[0]
    spread = fade[0]
    tri = iota((BLK, BLK), 0) - iota((BLK, BLK), 1)

    def one(raw, d, mask):
        rate = jax.nn.softplus(raw + params[d : d + 1, :])
        log = -jnp.exp(params[2 + d : 3 + d, :]) * rate + spread
        cum = jnp.dot(mask.astype(f32), log, precision=HIGH, preferred_element_type=f32)
        return rate, cum

    rate_f, cum_f = one(ahead[0], 0, tri >= 0)
    rate_b, cum_b = one(back[0], 1, tri <= 0)
    tot_f, tot_b = cum_f[BLK - 1 :], cum_b[:1]
    parts = (
        rate_f,
        rate_b,
        cum_f,
        cum_b,
        rate_f * jnp.exp(tot_f - cum_f),
        rate_b * jnp.exp(tot_b - cum_b),
        jnp.exp(cum_f),
        jnp.exp(cum_b),
    )
    gap = jnp.zeros((BLK, SLOT - STEP_HEADS), f32)
    rest = jnp.zeros((BLK, 128 - SLOT * len(parts)), f32)
    for g in range(steps):
        at = slice(g * STEP_HEADS, (g + 1) * STEP_HEADS)
        pieces = []
        for part in parts:
            pieces += [part[:, at], gap]
        packed = jnp.concatenate(pieces + [rest], axis=1)
        cols[g] = packed
        rows[g] = packed.T[: 4 * SLOT]
    totals[0:1] = tot_f
    totals[1:2] = tot_b


def expand(cols, which, width):
    pick = iota((128, width), 0) == which * SLOT + iota((128, width), 1) // HEAD_DIM
    return jnp.dot(cols, pick.astype(f32), precision=HIGH, preferred_element_type=f32)


def conv(ref, halo, taps):
    edge = halo[...].astype(f32)
    full = jnp.concatenate([edge[:8], ref[0].astype(f32), edge[8:]], axis=0)
    total = full[6 : 6 + BLK] * taps[0:1]
    for k in range(1, taps.shape[0]):
        total = total + full[6 + k : 6 + k + BLK] * taps[k : k + 1]
    return jax.nn.silu(total).astype(bf16)


def state_kernel(x, b, c, xh, bh, ch, xt, bt, ct, cols, xo, bo, co, uf, ub):
    xc, bc = conv(x, xh, xt), conv(b, bh, bt)
    xo[...] = xc
    bo[...] = bc
    co[...] = conv(c, ch, ct)
    width = xc.shape[1]
    half = width // 2
    packed = cols[0]
    xf = xc.astype(f32)
    for which, out in ((FF, uf), (FB, ub)):
        scaled = (xf * expand(packed, which, width)).astype(bf16)
        both = lax.dot_general(
            scaled, bc, (((0,), (0,)), ((), ())), preferred_element_type=f32
        )
        out[:half] = both[:half, :STATE].astype(bf16)
        out[half:] = both[half:, STATE:].astype(bf16)


def block_kernel(x, b, c, cols, rows, out):
    packed, across = cols[0], rows[0]
    ahead = iota((BLK, BLK), 1) - iota((BLK, BLK), 0)
    lower, upper = ahead < 0, ahead > 0
    lane = iota((BLK, 128), 1)
    scores = [
        lax.dot_general(
            c[:, i * STATE : (i + 1) * STATE],
            b[:, i * STATE : (i + 1) * STATE],
            (((1,), (1,)), ((), ())),
            preferred_element_type=f32,
        )
        for i in range(2)
    ]

    def head(j, pair):
        def col(a):
            return packed[:, a * SLOT + j : a * SLOT + j + 1]

        def row(a):
            return across[a * SLOT + j : a * SLOT + j + 1]

        gaps = jnp.where(lower, col(CF) - row(CF), col(CB) - row(CB))
        rate = jnp.where(lower, row(RF), jnp.where(upper, row(RB), row(RF) + row(RB)))
        weights = (scores[j * 2 // STEP_HEADS] * jnp.exp(gaps) * rate).astype(bf16)
        return jnp.dot(weights, pair, preferred_element_type=f32)

    for k in range(STEP_HEADS // 2):
        at = slice(k * 128, (k + 1) * 128)
        pair = x[:, at]
        out[:, at] = jnp.where(lane < HEAD_DIM, head(2 * k, pair), head(2 * k + 1, pair))


def finish_kernel(local, c, cols, sf, sb, gate, gain, out):
    packed = cols[0]
    width = local.shape[1]
    first = iota((BLK, width), 1) < width // 2
    y = local[...]
    for which, state in ((EF, sf), (EB, sb)):
        by_group = [
            lax.dot_general(
                c[:, i * STATE : (i + 1) * STATE],
                state[...],
                (((1,), (1,)), ((), ())),
                preferred_element_type=f32,
            )
            for i in range(2)
        ]
        y = y + jnp.where(first, by_group[0], by_group[1]) * expand(packed, which, width)
    gated = y.astype(bf16).astype(f32) * jax.nn.silu(gate[0].astype(f32))
    same = iota((width, width), 0) // HEAD_DIM == iota((width, width), 1) // HEAD_DIM
    mean = jnp.dot(
        gated * gated,
        jnp.where(same, 1.0 / HEAD_DIM, 0.0),
        precision=HIGH,
        preferred_element_type=f32,
    )
    out[0] = (gated * lax.rsqrt(mean + 1e-6) * gain[...].astype(f32)).astype(bf16)


def scan_kernel(uf, ub, decay, of, ob):
    count = uf.shape[0]
    state = jnp.zeros(uf.shape[1:], f32)
    for p in range(count):
        of[p] = state.astype(bf16)
        state = state * decay[0][:, p : p + 1] + uf[p].astype(f32)
    state = jnp.zeros(uf.shape[1:], f32)
    for p in reversed(range(count)):
        ob[p] = state.astype(bf16)
        state = state * decay[1][:, p : p + 1] + ub[p].astype(f32)


def scan_plain(u, decay, reverse):
    def step(state, piece):
        update, factor = piece
        return state * factor[:, None] + update.astype(f32), state.astype(bf16)

    return lax.scan(step, jnp.zeros(u.shape[1:], f32), (u, decay.T), reverse=reverse)[1]


def exchange(uf, ub, totals):
    count = lax.axis_size(ALL)
    heads = totals.shape[1]
    each = uf.shape[0] // count
    everyone = lax.all_gather(totals, ALL)
    mine = lax.axis_index(ALL) * each + jnp.arange(each)
    pick = (mine[:, None] // HEAD_DIM == jnp.arange(heads)[None]).astype(f32)
    decay = jnp.exp(jnp.einsum("rh,pdh->drp", pick, everyone, precision=HIGH))
    uf, ub = (
        lax.all_to_all(u, ALL, split_axis=0, concat_axis=0, tiled=True).reshape(
            count, each, STATE
        )
        for u in (uf, ub)
    )
    if count <= 64:
        shape = jax.ShapeDtypeStruct(uf.shape, bf16)
        sf, sb = pl.pallas_call(scan_kernel, out_shape=(shape, shape))(uf, ub, decay)
    else:
        sf, sb = scan_plain(uf, decay[0], False), scan_plain(ub, decay[1], True)
    return tuple(
        lax.all_to_all(
            s.reshape(count * each, STATE), ALL, split_axis=0, concat_axis=0, tiled=True
        )
        for s in (sf, sb)
    )


def local(x, b, c, gate, ahead, back, fade, x_taps, b_taps, c_taps, offsets, exponents, gain):
    tokens, x_width = x.shape[1:]
    b_width = b.shape[2]
    heads = ahead.shape[2]
    steps = heads // STEP_HEADS
    xs, bs = x_width // steps, b_width // steps
    wide, deep = lax.axis_size("sp"), lax.axis_size("dp")
    order = [s * deep + d for d in range(deep) for s in range(wide)]
    up = list(zip(order[:-1], order[1:]))
    down = [(target, source) for source, target in up]

    def edge(rows):
        return jnp.concatenate([x[0, rows], b[0, rows], c[0, rows]], axis=1)

    low = lax.ppermute(edge(slice(tokens - 2, tokens)), ("sp", "dp"), up)
    high = lax.ppermute(edge(slice(0, 1)), ("sp", "dp"), down)
    width = low.shape[1]
    halo = jnp.concatenate(
        [jnp.zeros((6, width), bf16), low, high, jnp.zeros((7, width), bf16)], axis=0
    )
    mine = [t.astype(f32) for t in (x_taps, b_taps, c_taps)]
    mine.append(jnp.concatenate([offsets, exponents], axis=0))
    bounds = [0]
    for piece in mine:
        bounds.append(bounds[-1] + piece.shape[1])
    gathered = lax.all_gather(jnp.concatenate(mine, axis=1), "sp")
    xt, bt, ct, params = (
        jnp.transpose(gathered[:, :, lo:hi], (1, 0, 2)).reshape(gathered.shape[1], -1)
        for lo, hi in zip(bounds[:-1], bounds[1:])
    )
    cols, rows, totals = pl.pallas_call(
        rates_kernel,
        out_shape=(
            jax.ShapeDtypeStruct((steps, BLK, 128), f32),
            jax.ShapeDtypeStruct((steps, 4 * SLOT, BLK), f32),
            jax.ShapeDtypeStruct((2, heads), f32),
        ),
    )(ahead, back, fade, params)

    def raw(size):
        return pl.BlockSpec((1, tokens, size), lambda g: (0, 0, g))

    def flat(rows_, size, start=0):
        return pl.BlockSpec((rows_, size), lambda g: (0, start + g))

    def stacked(rows_, size=128):
        return pl.BlockSpec((1, rows_, size), lambda g: (g, 0, 0))

    state_spec = pl.BlockSpec((xs, STATE), lambda g: (g, 0))
    taps = xt.shape[0]
    params_ = pltpu.CompilerParams(dimension_semantics=("arbitrary",))
    xc, bc, cc, uf, ub = pl.pallas_call(
        state_kernel,
        grid=(steps,),
        in_specs=[
            raw(xs),
            raw(bs),
            raw(bs),
            flat(16, xs),
            flat(16, bs, x_width // bs),
            flat(16, bs, (x_width + b_width) // bs),
            flat(taps, xs),
            flat(taps, bs),
            flat(taps, bs),
            stacked(BLK),
        ],
        out_specs=[flat(tokens, xs), flat(tokens, bs), flat(tokens, bs), state_spec, state_spec],
        out_shape=[
            jax.ShapeDtypeStruct((tokens, x_width), bf16),
            jax.ShapeDtypeStruct((tokens, b_width), bf16),
            jax.ShapeDtypeStruct((tokens, b_width), bf16),
            jax.ShapeDtypeStruct((x_width, STATE), bf16),
            jax.ShapeDtypeStruct((x_width, STATE), bf16),
        ],
        compiler_params=params_,
    )(x, b, c, halo, halo, halo, xt, bt, ct, cols)
    y = pl.pallas_call(
        block_kernel,
        grid=(steps,),
        in_specs=[
            flat(tokens, xs),
            flat(tokens, bs),
            flat(tokens, bs),
            stacked(BLK),
            stacked(4 * SLOT),
        ],
        out_specs=flat(tokens, xs),
        out_shape=jax.ShapeDtypeStruct((tokens, x_width), f32),
        compiler_params=params_,
    )(xc, bc, cc, cols, rows)
    sf, sb = exchange(uf, ub, totals)
    return pl.pallas_call(
        finish_kernel,
        grid=(steps,),
        in_specs=[
            flat(tokens, xs),
            flat(tokens, bs),
            stacked(BLK),
            state_spec,
            state_spec,
            raw(xs),
            flat(1, xs),
        ],
        out_specs=raw(xs),
        out_shape=jax.ShapeDtypeStruct(x.shape, bf16),
        compiler_params=params_,
    )(y, cc, cols, sf, sb, gate, gain[None])


def solution(mesh):
    token = P("dp", "sp", None)
    placed = (token,) * 7 + (P(None, "sp"),) * 5 + (P(),)
    return jax.shard_map(local, mesh=mesh, in_specs=placed, out_specs=token, check_vma=False)
```

profile of v0, /device:TPU:0, one launch (start us, length us, event | category | flops | bytes accessed | tf_op | source)
XLA Modules:
  0.0 183.8 jit_solution(17639351758969968331)
XLA Ops:
  0.0 0.8 slice_bitcast_fusion
  0.8 0.8 slice_bitcast_fusion.3
  1.6 1.3 collective-permute-start.1
  2.9 0.8 slice_bitcast_fusion.1
  3.8 0.8 slice_bitcast_fusion.5
  4.6 3.0 %collective-permute-start = (bf16[2,7168]{1,0:T(2,128)(2,1)S(1)}, bf16[2,7168]{1,0:T(2,128)(2,1)S(1)}, u32[]{:S(2)}, u32[]{:S(2)}) collective-permute-start(bf16[2,7168]{1,0:T(2,128)(2,1)S(1)} %pad_maximum_fusion), channel_id=1, source_target_pairs={{0,8},{8,16},{16,24},{24,1},{1,9},{9,17},{17,25},{25,2},{2,10},{10... | collective-permute-start | bytes 86024 | tf_op jit(solution)/shard_map/ppermute | solution.py:215
  7.6 0.7 convert_element_type.11
  8.3 0.7 convert_element_type.12
  9.0 0.7 convert_element_type.10
  9.7 0.7 maximum_bitcast_fusion
  10.4 8.3 %all-gather.2 = f32[4,4,1804]{2,1,0:T(4,128)S(1)} all-gather(f32[1,4,1804]{2,1,0:T(4,128)S(1)} %maximum_bitcast_fusion), channel_id=2, replica_groups=mesh['sp'=4,'dp'=8] {'sp'}, dimensions={0}, use_global_device_ids=true | all-gather | bytes 144320 | tf_op jit(solution)/shard_map/all_gather | solution.py:226
  18.7 0.6 fusion.4
  19.4 0.6 slice.40
  20.1 1.5 copy.27.ahead
  21.5 1.5 copy.28.back
  23.0 1.5 copy.29.fade
  24.4 0.7 reshape.68.params
  25.1 3.3 %shard_map.127 = (f32[8,128,128]{2,1,0:T(8,128)}, f32[8,32,128]{2,1,0:T(8,128)}, f32[2,48]{1,0:T(2,128)}) custom-call(f32[1,128,48]{2,1,0:T(8,128)} %copy.27.ahead, f32[1,128,48]{2,1,0:T(8,128)} %copy.28.back, f32[1,128,48]{2,1,0:T(8,128)} %copy.29.fade, f32[4,48]{1,0:T(4,128)} %reshape.68.params), custom_call_target="tpu_custom_call" | custom-call | tf_op jit(solution)/shard_map/pallas_call | solution.py:231
  28.5 0.8 maximum_maximum_fusion.xh.bh.ch
  29.3 12.0 %shard_map.128 = (bf16[128,3072]{1,0:T(8,128)(2,1)}, bf16[128,2048]{1,0:T(8,128)(2,1)}, bf16[128,2048]{1,0:T(8,128)(2,1)}, bf16[3072,128]{1,0:T(8,128)(2,1)}, bf16[3072,128]{1,0:T(8,128)(2,1)}) custom-call(bf16[1,128,3072]{2,1,0:T(8,128)(2,1)} %x.1, bf16[1,128,2048]{2,1,0:T(8,128)(2,1)} %b.1, bf16[1,128,2048]{2,1,0:T(8,128)(2,1)} %c.1, ...), custom_call_target="tpu_custom_call" | custom-call | tf_op jit(solution)/shard_map/pallas_call | solution.py:252
  41.3 25.7 %all_to_all.34.uf = bf16[32,96,128]{2,1,0:T(8,128)(2,1)} all-to-all(bf16[32,96,128]{2,1,0:T(8,128)(2,1)} %bitcast.36), channel_id=1, replica_groups=mesh['sp'=4,'dp'=8] {'dp','sp'}, dimensions={0} | all-to-all | bytes 1572864 | tf_op jit(solution)/shard_map/all_to_all | solution.py:183
  67.0 3.6 %all-to-all-start.1 = ((bf16[32,96,128]{2,1,0:T(8,128)(2,1)}), bf16[32,96,128]{2,1,0:T(8,128)(2,1)S(1)}, u32[]{:S(2)}, u32[]{:S(2)}) async-start(bf16[32,96,128]{2,1,0:T(8,128)(2,1)} %bitcast.15), calls=%async_computation.1 | async-start | bytes 1572864 | tf_op jit(solution)/shard_map/all_to_all | solution.py:183
  70.6 48.0 %all-gather.3 = f32[32,2,48]{2,1,0:T(2,128)S(1)} all-gather(f32[1,2,48]{2,1,0:T(2,128)S(1)} %bitcast.41), channel_id=3, replica_groups=mesh['sp'=4,'dp'=8] {'dp','sp'}, dimensions={0}, use_global_device_ids=true | all-gather | bytes 12672 | tf_op jit(solution)/shard_map/all_gather | solution.py:178
  118.8 0.7 copy.31
  119.5 0.9 copy-done.1
  120.5 3.4 %shard_map.130 = (bf16[32,96,128]{2,1,0:T(8,128)(2,1)}, bf16[32,96,128]{2,1,0:T(8,128)(2,1)}) custom-call(bf16[32,96,128]{2,1,0:T(8,128)(2,1)} %all_to_all.34.uf, bf16[32,96,128]{2,1,0:T(8,128)(2,1)} %copy-done.1, f32[2,96,32]{2,1,0:T(8,128)} %bitcast.37), custom_call_target="tpu_custom_call" | custom-call | tf_op jit(solution)/shard_map/pallas_call | solution.py:190
  123.9 24.0 %all_to_all.35 = bf16[32,96,128]{2,1,0:T(8,128)(2,1)} all-to-all(bf16[32,96,128]{2,1,0:T(8,128)(2,1)} %get-tuple-element.23), channel_id=1, replica_groups=mesh['sp'=4,'dp'=8] {'dp','sp'}, dimensions={0} | all-to-all | bytes 1572864 | tf_op jit(solution)/shard_map/all_to_all | solution.py:194
  147.9 3.5 %all-to-all-start.3 = ((bf16[32,96,128]{2,1,0:T(8,128)(2,1)}), bf16[32,96,128]{2,1,0:T(8,128)(2,1)S(1)}, u32[]{:S(2)}, u32[]{:S(2)}) async-start(bf16[32,96,128]{2,1,0:T(8,128)(2,1)} %get-tuple-element.24), calls=%async_computation.3 | async-start | bytes 1572864 | tf_op jit(solution)/shard_map/all_to_all | solution.py:194
  152.1 7.5 %shard_map.129.local = f32[128,3072]{1,0:T(8,128)} custom-call(bf16[128,3072]{1,0:T(8,128)(2,1)} %get-tuple-element.16.x, bf16[128,2048]{1,0:T(8,128)(2,1)} %get-tuple-element.17.b, bf16[128,2048]{1,0:T(8,128)(2,1)} %get-tuple-element.18.c, f32[8,128,128]{2,1,0:T(8,128)} %get-tuple-element.15.cols, f32[8,32,128]{2,1,0:T(8,128)} %get-tuple-element.19.rows), custom_call_target="tpu_custom_call" | custom-call | tf_op jit(solution)/shard_map/pallas_call | solution.py:277
  159.5 12.5 %all-to-all-done.3 = bf16[32,96,128]{2,1,0:T(8,128)(2,1)S(1)} async-done(((bf16[32,96,128]{2,1,0:T(8,128)(2,1)}), bf16[32,96,128]{2,1,0:T(8,128)(2,1)S(1)}, u32[]{:S(2)}, u32[]{:S(2)}) %all-to-all-start.3) | async-done | bytes 786464 | tf_op jit(solution)/shard_map/all_to_all | solution.py:194
  172.0 0.9 copy-done
  172.9 10.9 %shard_map.131 = bf16[1,128,3072]{2,1,0:T(8,128)(2,1)} custom-call(f32[128,3072]{1,0:T(8,128)} %shard_map.129.local, bf16[128,2048]{1,0:T(8,128)(2,1)} %get-tuple-element.18.c, f32[8,128,128]{2,1,0:T(8,128)} %get-tuple-element.15.cols, bf16[3072,128]{1,0:T(8,128)(2,1)} %bitcast.34, bf16[3072,128]{1,0:T(8,128)(2,1)} %bitcast.35, bf16[1,128,3072]{2,1,0:T(8,128)(2,1)} %gate.1, ...), custom_call_target="tpu_custom_call" | custom-call | tf_op jit(solution)/shard_map/pallas_call | solution.py:292
  (20 shorter events, 0.9 us)
Async XLA Ops:
  1.6 26.8 %collective-permute-start.1 = (bf16[1,7168]{1,0:T(2,128)(2,1)S(1)}, bf16[1,7168]{1,0:T(2,128)(2,1)S(1)}, u32[]{:S(2)}, u32[]{:S(2)}) collective-permute-start(bf16[1,7168]{1,0:T(2,128)(2,1)S(1)} %pad_maximum_fusion.1), channel_id=1, source_target_pairs={{8,0},{16,8},{24,16},{1,24},{9,1},{17,9},{25,17},{2,25},{10,2},{18... | collective-permute-start | bytes 43016 | tf_op jit(solution)/shard_map/ppermute | solution.py:216
  4.6 23.9 %collective-permute-start = (bf16[2,7168]{1,0:T(2,128)(2,1)S(1)}, bf16[2,7168]{1,0:T(2,128)(2,1)S(1)}, u32[]{:S(2)}, u32[]{:S(2)}) collective-permute-start(bf16[2,7168]{1,0:T(2,128)(2,1)S(1)} %pad_maximum_fusion), channel_id=1, source_target_pairs={{0,8},{8,16},{16,24},{24,1},{1,9},{9,17},{17,25},{25,2},{2,10},{10... | collective-permute-start | bytes 86024 | tf_op jit(solution)/shard_map/ppermute | solution.py:215
  41.3 29.3 %copy-start.3 = (f32[2,48]{1,0:T(2,128)S(1)}, f32[2,48]{1,0:T(2,128)}, u32[]{:S(2)}) copy-start(f32[2,48]{1,0:T(2,128)} %get-tuple-element.22) | copy-start | bytes 1156
  67.0 52.6 %all-to-all-start.1 = ((bf16[32,96,128]{2,1,0:T(8,128)(2,1)}), bf16[32,96,128]{2,1,0:T(8,128)(2,1)S(1)}, u32[]{:S(2)}, u32[]{:S(2)}) async-start(bf16[32,96,128]{2,1,0:T(8,128)(2,1)} %bitcast.15), calls=%async_computation.1 | async-start | bytes 1572864 | tf_op jit(solution)/shard_map/all_to_all | solution.py:183
  119.5 0.9 copy-start.1
  123.9 27.6 %copy-start.2 = (bf16[3072]{0:T(1024)(128)(2,1)S(1)}, bf16[3072]{0:T(1024)(128)(2,1)}, u32[]{:S(2)}) copy-start(bf16[3072]{0:T(1024)(128)(2,1)} %param.25) | copy-start | bytes 18436
  147.9 24.1 %all-to-all-start.3 = ((bf16[32,96,128]{2,1,0:T(8,128)(2,1)}), bf16[32,96,128]{2,1,0:T(8,128)(2,1)S(1)}, u32[]{:S(2)}, u32[]{:S(2)}) async-start(bf16[32,96,128]{2,1,0:T(8,128)(2,1)} %get-tuple-element.24), calls=%async_computation.3 | async-start | bytes 1572864 | tf_op jit(solution)/shard_map/all_to_all | solution.py:194
  172.0 0.9 copy-start
where the time goes:
time: 185 us; the launch traced here: 184 us
  blocking collectives  106 us (57%)
  Pallas kernels  37.1 us (20%)
  local copies, waits for them, and re-layouts  12.8 us (7%)
  waiting for transfers between devices  12.5 us (7%)
  starting transfers between devices  11.5 us (6%)
  other arithmetic  3.68 us (2%)
    all_gather x1, blocking collectives, exchange(): everyone = lax.all_gather(totals, ALL)  48 us
    all_to_all x1, blocking collectives, exchange(): lax.all_to_all(u, ALL, split_axis=0, concat_axis=0, tiled=True)  25.7 us
    all_to_all x1, blocking collectives, exchange(): lax.all_to_all(s.reshape(count * each, STATE), ALL, split_axis=0, concat_...  24 us
    all_to_all x1, waiting for transfers between devices, exchange(): lax.all_to_all(s.reshape(count * each, STATE), ALL, split_axis=0, concat_...  12.5 us
    pallas_call x1, Pallas kernels, local(): pl.pallas_call(state_kernel, grid=(steps,), in_specs=[raw(xs), raw(bs), r...  12 us
    pallas_call x1, Pallas kernels, local(): pl.pallas_call(finish_kernel, grid=(steps,), in_specs=[flat(tokens, xs),...  10.9 us
    all_gather x1, blocking collectives, local(): gathered = lax.all_gather(jnp.concatenate(mine, axis=1), 'sp')  8.29 us
    pallas_call x1, Pallas kernels, local(): pl.pallas_call(block_kernel, grid=(steps,), in_specs=[flat(tokens, xs), f...  7.47 us
  transfers between devices with their start and end apart: 4, of which 1 were waited for; matrix products, arithmetic and copies ran while one was open for 7% of the time, Pallas kernels for 6%

commit v1 on v0

--- a/solution.py
+++ b/solution.py
@@ -54,9 +54,11 @@
             pieces += [part[:, at], gap]
         packed = jnp.concatenate(pieces + [rest], axis=1)
         cols[g] = packed
-        rows[g] = packed.T[: 4 * SLOT]
-    totals[0:1] = tot_f
-    totals[1:2] = tot_b
+        turned = packed.T[: 4 * SLOT]
+        rows[g] = turned
+        for d, (start, end) in enumerate(((CF * SLOT, BLK - 1), (CB * SLOT, 0))):
+            last = turned[start : start + STEP_HEADS, end : end + 1]
+            totals[d, at] = jnp.broadcast_to(last, (STEP_HEADS, 128))
 
 
 def expand(cols, which, width):
@@ -73,7 +75,7 @@
     return jax.nn.silu(total).astype(bf16)
 
 
-def state_kernel(x, b, c, xh, bh, ch, xt, bt, ct, cols, xo, bo, co, uf, ub):
+def state_kernel(place, x, b, c, xh, bh, ch, xt, bt, ct, cols, xo, bo, co, send, keep):
     xc, bc = conv(x, xh, xt), conv(b, bh, bt)
     xo[...] = xc
     bo[...] = bc
@@ -82,13 +84,21 @@
     half = width // 2
     packed = cols[0]
     xf = xc.astype(f32)
-    for which, out in ((FF, uf), (FB, ub)):
+    both = []
+    for which in (FF, FB):
         scaled = (xf * expand(packed, which, width)).astype(bf16)
-        both = lax.dot_general(
+        full = lax.dot_general(
             scaled, bc, (((0,), (0,)), ((), ())), preferred_element_type=f32
         )
-        out[:half] = both[:half, :STATE].astype(bf16)
-        out[half:] = both[half:, STATE:].astype(bf16)
+        both.append((full[:half, :STATE].astype(bf16), full[half:, STATE:].astype(bf16)))
+
+    def put(out):
+        for d in range(2):
+            out[d, :half], out[d, half:] = both[d]
+
+    turn = pl.program_id(0)
+    pl.when(turn < pl.num_programs(0) // 2)(lambda: put(send))
+    pl.when(turn >= pl.num_programs(0) // 2)(lambda: put(keep))
 
 
 def block_kernel(x, b, c, cols, rows, out):
@@ -124,16 +134,18 @@
         out[:, at] = jnp.where(lane < HEAD_DIM, head(2 * k, pair), head(2 * k + 1, pair))
 
 
-def finish_kernel(local, c, cols, sf, sb, gate, gain, out):
+def finish_kernel(place, local, c, cols, mine, theirs, gate, gain, out):
+    own = pl.program_id(0) < pl.num_programs(0) // 2
     packed = cols[0]
     width = local.shape[1]
     first = iota((BLK, width), 1) < width // 2
     y = local[...]
-    for which, state in ((EF, sf), (EB, sb)):
+    for d, which in enumerate((EF, EB)):
+        state = jnp.where(own, mine[d], theirs[d])
         by_group = [
             lax.dot_general(
                 c[:, i * STATE : (i + 1) * STATE],
-                state[...],
+                state,
                 (((1,), (1,)), ((), ())),
                 preferred_element_type=f32,
             )
@@ -198,6 +210,127 @@
     )
 
 
+def pair_kernel(place, mine, theirs, own, par, send, keep):
+    early, fwd = place[0] == 0, place[1] == 1
+    e_own, e_par = jnp.exp(own[...]), jnp.exp(par[...])
+    scale_mine = (jnp.where(early, e_par[0], 1.0), jnp.where(early, 1.0, e_par[1]))
+    scale_theirs = (jnp.where(early, 1.0, e_own[0]), jnp.where(early, e_own[1], 1.0))
+    for h in range(own.shape[1]):
+        at = slice(h * HEAD_DIM, (h + 1) * HEAD_DIM)
+        f, b = (
+            mine[d, at].astype(f32) * scale_mine[d][h : h + 1]
+            + theirs[d, at].astype(f32) * scale_theirs[d][h : h + 1]
+            for d in range(2)
+        )
+        keep[at] = jnp.where(fwd, f, b).astype(bf16)
+        send[at] = jnp.where(fwd, b, f).astype(bf16)
+
+
+def segment_kernel(place, keep, got, pair, xpair, out):
+    fwd = place[1] == 1
+    here = jnp.where(fwd, pair[0], pair[1])
+    there = jnp.where(fwd, xpair[0], xpair[1])
+    factor, total = jnp.exp(here), jnp.exp(here + there)
+    high = total.astype(bf16)
+    middle = (total - high.astype(f32)).astype(bf16)
+    lowest = (total - high.astype(f32) - middle.astype(f32)).astype(bf16)
+    parts = [part.astype(f32) for part in (high, middle, lowest)]
+    chunks = out.shape[0]
+    each = pair.shape[1] // chunks
+    rows = each * HEAD_DIM
+    for j in range(chunks):
+        lines = []
+        for i in range(each):
+            h = j * each + i
+            at = slice(h * HEAD_DIM, (h + 1) * HEAD_DIM)
+            new = keep[at].astype(f32) + got[at].astype(f32) * factor[h : h + 1]
+            out[j, i * HEAD_DIM : (i + 1) * HEAD_DIM] = new.astype(bf16)
+            lines += [part[h : h + 1] for part in parts]
+        lines.append(jnp.zeros((out.shape[1] - rows - len(lines), STATE), f32))
+        out[j, rows:] = jnp.concatenate(lines, axis=0).astype(bf16)
+
+
+def carry_kernel(place, v, out):
+    fwd = place[1] == 1
+    count, rows = out.shape[:2]
+    each = rows // HEAD_DIM
+    state = [jnp.zeros((HEAD_DIM, STATE), f32)] * each
+    for i in range(count):
+        q = jnp.where(fwd, i, count - 1 - i)
+        piece = v[q].astype(f32)
+        lines = piece[rows:]
+        for h in range(each):
+            at = slice(h * HEAD_DIM, (h + 1) * HEAD_DIM)
+            out[q, at] = state[h].astype(bf16)
+            factor = lines[3 * h : 3 * h + 1] + lines[3 * h + 1 : 3 * h + 2]
+            factor = factor + lines[3 * h + 2 : 3 * h + 3]
+            state[h] = state[h] * factor + piece[at]
+
+
+def enter_kernel(place, entry, other, got, mine, theirs, own, par, xpair, keep, send):
+    early, fwd = place[0] == 0, place[1] == 1
+    e_own, e_par = jnp.exp(own[...]), jnp.exp(par[...])
+    past = jnp.exp(jnp.where(fwd, xpair[0], xpair[1]))
+    for h in range(own.shape[1]):
+        at = slice(h * HEAD_DIM, (h + 1) * HEAD_DIM)
+        line = slice(h, h + 1)
+        near = entry[at].astype(f32) * past[line] + got[at].astype(f32)
+        far = other[at].astype(f32)
+        f, b = jnp.where(fwd, near, far), jnp.where(fwd, far, near)
+        f_mine = f * e_par[0, line] + theirs[0, at].astype(f32)
+        b_mine = b * e_par[1, line] + theirs[1, at].astype(f32)
+        f_theirs = f * e_own[0, line] + mine[0, at].astype(f32)
+        b_theirs = b * e_own[1, line] + mine[1, at].astype(f32)
+        keep[0, at] = jnp.where(early, f, f_mine).astype(bf16)
+        keep[1, at] = jnp.where(early, b_mine, b).astype(bf16)
+        send[0, at] = jnp.where(early, f_theirs, f).astype(bf16)
+        send[1, at] = jnp.where(early, b, b_theirs).astype(bf16)
+
+
+def swap(a, bit):
+    wide, deep = lax.axis_size("sp"), lax.axis_size("dp")
+    perm = [
+        (s * deep + d, (s ^ bit) * deep + d) for s in range(wide) for d in range(deep)
+    ]
+    return lax.ppermute(a, ("sp", "dp"), perm)
+
+
+def run(kernel, shapes, place, *args):
+    smem = pl.BlockSpec(memory_space=pltpu.SMEM)
+    vmem = pl.BlockSpec(memory_space=pltpu.VMEM)
+    return pl.pallas_call(
+        kernel,
+        in_specs=[smem] + [vmem] * len(args),
+        out_shape=[jax.ShapeDtypeStruct(shape, bf16) for shape in shapes],
+    )(place, *args)
+
+
+def exchange_tree(send, keep, logs, place):
+    deep = lax.axis_size("dp")
+    half = logs.shape[1] // 2
+    whole_par = swap(logs, 1)
+    whole_pair = logs + whole_par
+    whole_xpair = swap(whole_pair, 2)
+    own, par, pair, xpair = (
+        lax.dynamic_slice_in_dim(a, place[0] * half, half, axis=1)
+        for a in (logs, whole_par, whole_pair, whole_xpair)
+    )
+    theirs = swap(send, 1)
+    rows = keep.shape[1:]
+    across, stay = run(pair_kernel, (rows, rows), place, keep, theirs, own, par)
+    got = swap(across, 2)
+    each = rows[0] // deep
+    (packed,) = run(segment_kernel, ((deep, each + 16, STATE),), place, stay, got, pair, xpair)
+    packed = lax.all_to_all(packed, "dp", split_axis=0, concat_axis=0)
+    (entry,) = run(carry_kernel, ((deep, each, STATE),), place, packed)
+    entry = lax.all_to_all(entry, "dp", split_axis=0, concat_axis=0).reshape(rows)
+    other = swap(entry, 2)
+    mine, back = run(
+        enter_kernel, (keep.shape,) * 2, place, entry, other, got, keep, theirs, own, par, xpair
+    )
+    return mine, swap(back, 1)
+
+
 def local(x, b, c, gate, ahead, back, fade, x_taps, b_taps, c_taps, offsets, exponents, gain):
     tokens, x_width = x.shape[1:]
     b_width = b.shape[2]
@@ -233,7 +366,7 @@
         out_shape=(
             jax.ShapeDtypeStruct((steps, BLK, 128), f32),
             jax.ShapeDtypeStruct((steps, 4 * SLOT, BLK), f32),
-            jax.ShapeDtypeStruct((2, heads), f32),
+            jax.ShapeDtypeStruct((2, heads, 128), f32),
         ),
     )(ahead, back, fade, params)
 
@@ -246,13 +379,47 @@
     def stacked(rows_, size=128):
         return pl.BlockSpec((1, rows_, size), lambda g: (g, 0, 0))
 
-    state_spec = pl.BlockSpec((xs, STATE), lambda g: (g, 0))
     taps = xt.shape[0]
     params_ = pltpu.CompilerParams(dimension_semantics=("arbitrary",))
-    xc, bc, cc, uf, ub = pl.pallas_call(
+    tree = wide == 4 and heads % (2 * deep) == 0 and 3 * heads // (2 * deep) <= 16
+    if tree:
+        spot = lax.axis_index("sp")
+        place = jnp.stack([spot % 2, spot // 2]).astype(jnp.int32)
+    else:
+        place = jnp.zeros((2,), jnp.int32)
+    middle = steps // 2
+
+    def shifted(spec, late):
+        index = spec.index_map
+
+        def move(g, place):
+            return index((g + middle * jnp.where(late, 1 - place[0], place[0])) % steps)
+
+        return pl.BlockSpec(spec.block_shape, move)
+
+    def sided(first):
+        def move(g, place):
+            return (0, jnp.minimum(g, middle - 1) if first else jnp.maximum(g - middle, 0), 0)
+
+        return pl.BlockSpec((2, xs, STATE), move)
+
+    def half_call(kernel, ins, in_sides, outs, out_sides, late, shapes):
+        return pl.pallas_call(
+            kernel,
+            grid_spec=pltpu.PrefetchScalarGridSpec(
+                num_scalar_prefetch=1,
+                grid=(steps,),
+                in_specs=[shifted(spec, late) for spec in ins[:in_sides[0]]]
+                + [sided(first) for first in in_sides[1]]
+                + [shifted(spec, late) for spec in ins[in_sides[0] :]],
+                out_specs=[shifted(spec, late) for spec in outs] + [sided(f) for f in out_sides],
+            ),
+            out_shape=shapes,
+            compiler_params=params_,
+        )
+    xc, bc, cc, send, keep = half_call(
         state_kernel,
-        grid=(steps,),
-        in_specs=[
+        [
             raw(xs),
             raw(bs),
             raw(bs),
@@ -264,16 +431,18 @@
             flat(taps, bs),
             stacked(BLK),
         ],
-        out_specs=[flat(tokens, xs), flat(tokens, bs), flat(tokens, bs), state_spec, state_spec],
-        out_shape=[
+        (10, ()),
+        [flat(tokens, xs), flat(tokens, bs), flat(tokens, bs)],
+        (True, False),
+        True,
+        [
             jax.ShapeDtypeStruct((tokens, x_width), bf16),
             jax.ShapeDtypeStruct((tokens, b_width), bf16),
             jax.ShapeDtypeStruct((tokens, b_width), bf16),
-            jax.ShapeDtypeStruct((x_width, STATE), bf16),
-            jax.ShapeDtypeStruct((x_width, STATE), bf16),
+            jax.ShapeDtypeStruct((2, x_width // 2, STATE), bf16),
+            jax.ShapeDtypeStruct((2, x_width // 2, STATE), bf16),
         ],
-        compiler_params=params_,
-    )(x, b, c, halo, halo, halo, xt, bt, ct, cols)
+    )(place, x, b, c, halo, halo, halo, xt, bt, ct, cols)
     y = pl.pallas_call(
         block_kernel,
         grid=(steps,),
@@ -288,23 +457,22 @@
         out_shape=jax.ShapeDtypeStruct((tokens, x_width), f32),
         compiler_params=params_,
     )(xc, bc, cc, cols, rows)
-    sf, sb = exchange(uf, ub, totals)
-    return pl.pallas_call(
+    if tree:
+        mine, theirs = exchange_tree(send, keep, totals, place)
+    else:
+        uf, ub = (jnp.concatenate([keep[d], send[d]], axis=0) for d in range(2))
+        states = jnp.stack(exchange(uf, ub, totals[:, :, 0]))
+        mine, theirs = states[:, : x_width // 2], states[:, x_width // 2 :]
+    (out,) = half_call(
         finish_kernel,
-        grid=(steps,),
-        in_specs=[
-            flat(tokens, xs),
-            flat(tokens, bs),
-            stacked(BLK),
-            state_spec,
-            state_spec,
-            raw(xs),
-            flat(1, xs),
-        ],
-        out_specs=raw(xs),
-        out_shape=jax.ShapeDtypeStruct(x.shape, bf16),
-        compiler_params=params_,
-    )(y, cc, cols, sf, sb, gate, gain[None])
+        [flat(tokens, xs), flat(tokens, bs), stacked(BLK), raw(xs), flat(1, xs)],
+        (3, (True, False)),
+        [raw(xs)],
+        (),
+        False,
+        [jax.ShapeDtypeStruct(x.shape, bf16)],
+    )(place, y, cc, cols, mine, theirs, gate, gain[None])
+    return out
 
 
 def solution(mesh):

time: 185 us -> 139 us (0.75)
  blocking collectives: 106 us -> 42.8 us
  Pallas kernels: 37.1 us -> 48.5 us
  waiting for transfers between devices: 12.5 us -> 19.5 us
  starting transfers between devices: 11.5 us -> 6.92 us
  local copies, waits for them, and re-layouts: 12.8 us -> 15.9 us
    all_gather x1 -> x0, blocking collectives: 48 us -> none  [exchange(): everyone = lax.all_gather(totals, ALL)]
    ppermute x0 -> x6, waiting for transfers between devices: none -> 19.5 us  [swap(): return lax.ppermute(a, ('sp', 'dp'), perm)]
    all_to_all x2, blocking collectives: 49.7 us -> 34.4 us  [the longest x1 19.4 us: exchange_tree(): packed = lax.all_to_all(packed, 'dp', split_axis=0, concat_axis=0)]
    all_to_all x2 -> x0, waiting for transfers between devices: 12.5 us -> none  [the longest x1 12.5 us: exchange(): lax.all_to_all(s.reshape(count * each, STATE), ALL, split_axis=0, concat_...]
    pallas_call x3 -> x6, Pallas kernels: 26.3 us -> 37.3 us  [the longest x1 14.9 us: local(): half_call(state_kernel, [raw(xs), raw(bs), raw(bs), flat(16, xs), flat(16...]
    all_to_all x2 -> x0, starting transfers between devices: 7.16 us -> none  [the longest x1 3.62 us: exchange(): lax.all_to_all(u, ALL, split_axis=0, concat_axis=0, tiled=True)]
    ppermute x0 -> x6, starting transfers between devices: none -> 3.23 us  [swap(): return lax.ppermute(a, ('sp', 'dp'), perm)]
    dynamic_slice x0 -> x4, local copies, waits for them, and re-layouts: none -> 2.41 us  [exchange_tree(): lax.dynamic_slice_in_dim(a, place[0] * half, half, axis=1)]
  transfers between devices with their start and end apart: 4 -> 8, of which waited for: 1 -> 3; matrix products, arithmetic and copies ran while one was open for 7% -> 10% of each run, Pallas kernels for 6% -> 8%
where the time goes in v1:
time: 139 us; the launch traced here: 138 us
  Pallas kernels  48.5 us (35%)
  blocking collectives  42.8 us (31%)
  waiting for transfers between devices  19.5 us (14%)
  local copies, waits for them, and re-layouts  15.9 us (11%)
  starting transfers between devices  6.92 us (5%)
  other arithmetic  4.32 us (3%)
    ppermute x6, waiting for transfers between devices, swap(): return lax.ppermute(a, ('sp', 'dp'), perm)  19.5 us
    all_to_all x1, blocking collectives, exchange_tree(): packed = lax.all_to_all(packed, 'dp', split_axis=0, concat_axis=0)  19.4 us
    all_to_all x1, blocking collectives, exchange_tree(): lax.all_to_all(entry, 'dp', split_axis=0, concat_axis=0).reshape(rows)  15 us
    pallas_call x1, Pallas kernels, local(): half_call(state_kernel, [raw(xs), raw(bs), raw(bs), flat(16, xs), flat(16...  14.9 us
    pallas_call x1, Pallas kernels, local(): half_call(finish_kernel, [flat(tokens, xs), flat(tokens, bs), stacked(BLK...  12.3 us
    pallas_call x4, Pallas kernels, run(): pl.pallas_call(kernel, in_specs=[smem] + [vmem] * len(args), out_shape=[j...  10.1 us
    all_gather x1, blocking collectives, local(): gathered = lax.all_gather(jnp.concatenate(mine, axis=1), 'sp')  8.34 us
    unnamed x17, local copies, waits for them, and re-layouts  7.69 us
  transfers between devices with their start and end apart: 8, of which 3 were waited for; matrix products, arithmetic and copies ran while one was open for 10% of the time, Pallas kernels for 8%

profile of v1, /device:TPU:0, one launch (start us, length us, event | category | flops | bytes accessed | tf_op | source)
XLA Modules:
  0.0 138.0 jit_solution(6416908683283754249)
XLA Ops:
  0.0 0.8 slice_bitcast_fusion.1
  0.8 0.8 slice_bitcast_fusion.5
  1.7 2.4 %collective-permute-start = (bf16[2,7168]{1,0:T(2,128)(2,1)S(1)}, bf16[2,7168]{1,0:T(2,128)(2,1)S(1)}, u32[]{:S(2)}, u32[]{:S(2)}) collective-permute-start(bf16[2,7168]{1,0:T(2,128)(2,1)S(1)} %pad_maximum_fusion), channel_id=1, source_target_pairs={{0,8},{8,16},{16,24},{24,1},{1,9},{9,17},{17,25},{25,2},{2,10},{10... | collective-permute-start | bytes 86024 | tf_op jit(solution)/shard_map/ppermute | solution.py:348
  4.1 0.8 slice_bitcast_fusion.3
  4.9 0.8 slice_bitcast_fusion
  5.7 1.3 collective-permute-start.1
  7.0 0.7 convert_element_type.9
  7.7 0.7 convert_element_type.10
  9.1 0.7 maximum_bitcast_fusion
  9.8 8.3 %all-gather.1 = f32[4,4,1804]{2,1,0:T(4,128)S(1)} all-gather(f32[1,4,1804]{2,1,0:T(4,128)S(1)} %maximum_bitcast_fusion), channel_id=2, replica_groups=mesh['sp'=4,'dp'=8] {'sp'}, dimensions={0}, use_global_device_ids=true | all-gather | bytes 144320 | tf_op jit(solution)/shard_map/all_gather | solution.py:359
  20.7 1.5 %copy.19.ahead = f32[1,128,48]{2,1,0:T(8,128)} copy(f32[1,128,48]{1,2,0:T(8,128)} %param.17) | data formatting | bytes 49152 | tf_op args[4]
  22.2 1.5 %copy.20.back = f32[1,128,48]{2,1,0:T(8,128)} copy(f32[1,128,48]{1,2,0:T(8,128)} %param.18) | data formatting | bytes 49152 | tf_op args[5]
  23.6 1.5 %copy.21.fade = f32[1,128,48]{2,1,0:T(8,128)} copy(f32[1,128,48]{1,2,0:T(8,128)} %param.19) | data formatting | bytes 49152 | tf_op args[6]
  25.2 3.7 %shard_map.127 = (f32[8,128,128]{2,1,0:T(8,128)}, f32[8,32,128]{2,1,0:T(8,128)}, f32[2,48,128]{2,1,0:T(8,128)}) custom-call(f32[1,128,48]{2,1,0:T(8,128)} %copy.19.ahead, f32[1,128,48]{2,1,0:T(8,128)} %copy.20.back, f32[1,128,48]{2,1,0:T(8,128)} %copy.21.fade, f32[4,48]{1,0:T(4,128)} %reshape.18.params), custom_call_target="tpu_custom_call" | custom-call | tf_op jit(solution)/shard_map/pallas_call | solution.py:364
  28.9 0.8 maximum_maximum_fusion.xh.bh.ch
  29.7 14.9 %shard_map.128 = (bf16[128,3072]{1,0:T(8,128)(2,1)}, bf16[128,2048]{1,0:T(8,128)(2,1)}, bf16[128,2048]{1,0:T(8,128)(2,1)}, bf16[2,1536,128]{2,1,0:T(8,128)(2,1)}, bf16[2,1536,128]{2,1,0:T(8,128)(2,1)}) custom-call(s32[2]{0:T(128)} %pad_add_fusion.place, bf16[1,128,3072]{2,1,0:T(8,128)(2,1)} %x.1, bf16[1,128,2048]{2,1,0:T(8,128)(2,1)} %b.1, ...), custom_call_target="tpu_custom_call" | custom-call | tf_op jit(solution)/shard_map/pallas_call | solution.py:420
  45.8 1.5 %collective-permute-done.3 = f32[2,48,128]{2,1,0:T(8,128)S(1)} collective-permute-done((f32[2,48,128]{2,1,0:T(8,128)S(1)}, f32[2,48,128]{2,1,0:T(8,128)S(1)}, u32[]{:S(2)}, u32[]{:S(2)}) %collective-permute-start.3) | collective-permute-done | bytes 49184 | tf_op jit(solution)/shard_map/ppermute | solution.py:295
  47.8 0.9 copy-done
  48.7 2.6 %shard_map.130 = (bf16[1536,128]{1,0:T(8,128)(2,1)}, bf16[1536,128]{1,0:T(8,128)(2,1)}) custom-call(s32[2]{0:T(128)} %pad_add_fusion.place, bf16[2,1536,128]{2,1,0:T(8,128)(2,1)} %get-tuple-element.22.mine, bf16[2,1536,128]{2,1,0:T(8,128)(2,1)} %copy-done, f32[2,24,128]{2,1,0:T(8,128)} %constant_dynamic-slice_fusion.3.own, ...), custom_call_target="tpu_custom_call" | custom-call | tf_op jit(solution)/shard_map/pallas_call | solution.py:301
  51.4 1.9 %collective-permute-start.4 = (bf16[1536,128]{1,0:T(8,128)(2,1)}, bf16[1536,128]{1,0:T(8,128)(2,1)S(1)}, u32[]{:S(2)}, u32[]{:S(2)}) collective-permute-start(bf16[1536,128]{1,0:T(8,128)(2,1)} %get-tuple-element.26), channel_id=1, source_target_pairs={{0,16},{1,17},{2,18},{3,19},{4,20},{5,21},{6,22},{7,23},{8,24},{9,... | collective-permute-start | bytes 1179656 | tf_op jit(solution)/shard_map/ppermute | solution.py:295
  54.0 10.1 %collective-permute-done.5 = f32[2,48,128]{2,1,0:T(8,128)S(1)} collective-permute-done((f32[2,48,128]{2,1,0:T(8,128)S(1)}, f32[2,48,128]{2,1,0:T(8,128)S(1)}, u32[]{:S(2)}, u32[]{:S(2)}) %collective-permute-start.5) | collective-permute-done | bytes 49184 | tf_op jit(solution)/shard_map/ppermute | solution.py:295
  64.8 0.7 copy-done.1
  65.5 2.1 %shard_map.131 = bf16[8,208,128]{2,1,0:T(8,128)(2,1)} custom-call(s32[2]{0:T(128)} %pad_add_fusion.place, bf16[1536,128]{1,0:T(8,128)(2,1)} %get-tuple-element.25.keep, bf16[1536,128]{1,0:T(8,128)(2,1)} %copy-done.1, f32[2,24,128]{2,1,0:T(8,128)} %constant_dynamic-slice_fusion.1.pair, f32[2,24,128]{2,1,0:T(8,128)} %constant_dynamic-slice_fusion.xpair), custom_call_target="tpu_custom_call" | custom-call | tf_op jit(solution)/shard_map/pallas_call | solution.py:301
  67.6 19.4 %all_to_all.10.v = bf16[8,208,128]{2,1,0:T(8,128)(2,1)} all-to-all(bf16[8,208,128]{2,1,0:T(8,128)(2,1)} %shard_map.131), channel_id=1, replica_groups=mesh['sp'=4,'dp'=8] {'dp'}, dimensions={0} | all-to-all | bytes 851968 | tf_op jit(solution)/shard_map/all_to_all | solution.py:324
  87.0 1.9 %shard_map.132 = bf16[8,192,128]{2,1,0:T(8,128)(2,1)} custom-call(s32[2]{0:T(128)} %pad_add_fusion.place, bf16[8,208,128]{2,1,0:T(8,128)(2,1)} %all_to_all.10.v), custom_call_target="tpu_custom_call" | custom-call | tf_op jit(solution)/shard_map/pallas_call | solution.py:301
  88.9 15.0 %all_to_all.11 = bf16[8,192,128]{2,1,0:T(8,128)(2,1)S(1)} all-to-all(bf16[8,192,128]{2,1,0:T(8,128)(2,1)} %shard_map.132), channel_id=1, replica_groups=mesh['sp'=4,'dp'=8] {'dp'}, dimensions={0} | all-to-all | bytes 786432 | tf_op jit(solution)/shard_map/all_to_all | solution.py:326
  104.5 7.9 %collective-permute-done.6.other = bf16[1536,128]{1,0:T(8,128)(2,1)S(1)} collective-permute-done((bf16[1536,128]{1,0:T(8,128)(2,1)S(1)}, bf16[1536,128]{1,0:T(8,128)(2,1)S(1)}, u32[]{:S(2)}, u32[]{:S(2)}) %collective-permute-start.6) | collective-permute-done | bytes 393248 | tf_op jit(solution)/shard_map/ppermute | solution.py:295
  112.4 0.8 copy-done.4
  113.2 3.6 %shard_map.133 = (bf16[2,1536,128]{2,1,0:T(8,128)(2,1)}, bf16[2,1536,128]{2,1,0:T(8,128)(2,1)}) custom-call(s32[2]{0:T(128)} %pad_add_fusion.place, bf16[1536,128]{1,0:T(8,128)(2,1)} %bitcast.29, bf16[1536,128]{1,0:T(8,128)(2,1)} %copy-done.4, bf16[1536,128]{1,0:T(8,128)(2,1)} %copy-done.1, bf16[2,1536,128]{2,1,0:T(8,128)(2,1)} %get-tuple-element.22.mine, ...), custom_call_target="tpu_custom_call" | custom-call | tf_op jit(solution)/shard_map/pallas_call | solution.py:301
  117.3 7.5 %shard_map.129.local = f32[128,3072]{1,0:T(8,128)} custom-call(bf16[128,3072]{1,0:T(8,128)(2,1)} %get-tuple-element.18.x, bf16[128,2048]{1,0:T(8,128)(2,1)} %get-tuple-element.19.b, bf16[128,2048]{1,0:T(8,128)(2,1)} %get-tuple-element.20.c, f32[8,128,128]{2,1,0:T(8,128)} %get-tuple-element.17.cols, f32[8,32,128]{2,1,0:T(8,128)} %get-tuple-element.21.rows), custom_call_target="tpu_custom_call" | custom-call | tf_op jit(solution)/shard_map/pallas_call | solution.py:446
  124.8 0.9 copy-done.3
  125.7 12.3 %shard_map.134 = bf16[1,128,3072]{2,1,0:T(8,128)(2,1)} custom-call(s32[2]{0:T(128)} %pad_add_fusion.place, f32[128,3072]{1,0:T(8,128)} %shard_map.129.local, bf16[128,2048]{1,0:T(8,128)(2,1)} %get-tuple-element.20.c, f32[8,128,128]{2,1,0:T(8,128)} %get-tuple-element.17.cols, bf16[2,1536,128]{2,1,0:T(8,128)(2,1)} %get-tuple-element.27.mine, ...), custom_call_target="tpu_custom_call" | custom-call | tf_op jit(solution)/shard_map/pallas_call | solution.py:466
  (39 shorter events, 7.8 us)
Async XLA Ops:
  1.7 27.2 %collective-permute-start = (bf16[2,7168]{1,0:T(2,128)(2,1)S(1)}, bf16[2,7168]{1,0:T(2,128)(2,1)S(1)}, u32[]{:S(2)}, u32[]{:S(2)}) collective-permute-start(bf16[2,7168]{1,0:T(2,128)(2,1)S(1)} %pad_maximum_fusion), channel_id=1, source_target_pairs={{0,8},{8,16},{16,24},{24,1},{1,9},{9,17},{17,25},{25,2},{2,10},{10... | collective-permute-start | bytes 86024 | tf_op jit(solution)/shard_map/ppermute | solution.py:348
  5.7 23.1 %collective-permute-start.1 = (bf16[1,7168]{1,0:T(2,128)(2,1)S(1)}, bf16[1,7168]{1,0:T(2,128)(2,1)S(1)}, u32[]{:S(2)}, u32[]{:S(2)}) collective-permute-start(bf16[1,7168]{1,0:T(2,128)(2,1)S(1)} %pad_maximum_fusion.1), channel_id=1, source_target_pairs={{8,0},{16,8},{24,16},{1,24},{9,1},{17,9},{25,17},{2,25},{10,2},{18... | collective-permute-start | bytes 43016 | tf_op jit(solution)/shard_map/ppermute | solution.py:349
  29.7 15.3 %copy-start.5 = (f32[2,48,128]{2,1,0:T(8,128)S(1)}, f32[2,48,128]{2,1,0:T(8,128)}, u32[]{:S(2)}) copy-start(f32[2,48,128]{2,1,0:T(8,128)} %get-tuple-element.24) | copy-start | bytes 147460
  44.6 3.2 %collective-permute-start.2 = (bf16[2,1536,128]{2,1,0:T(8,128)(2,1)}, bf16[2,1536,128]{2,1,0:T(8,128)(2,1)S(1)}, u32[]{:S(2)}, u32[]{:S(2)}) collective-permute-start(bf16[2,1536,128]{2,1,0:T(8,128)(2,1)} %get-tuple-element.23), channel_id=1, source_target_pairs={{0,8},{1,9},{2,10},{3,11},{4,12},{5,13},{6,14},{7,15},{8,0},{9,1},... | collective-permute-start | bytes 2359304 | tf_op jit(solution)/shard_map/ppermute | solution.py:295
  45.0 2.2 %collective-permute-start.3 = (f32[2,48,128]{2,1,0:T(8,128)S(1)}, f32[2,48,128]{2,1,0:T(8,128)S(1)}, u32[]{:S(2)}, u32[]{:S(2)}) collective-permute-start(f32[2,48,128]{2,1,0:T(8,128)S(1)} %copy-done.5), channel_id=1, source_target_pairs={{0,8},{1,9},{2,10},{3,11},{4,12},{5,13},{6,14},{7,15},{8,0},{9,1},... | collective-permute-start | bytes 147464 | tf_op jit(solution)/shard_map/ppermute | solution.py:295
  47.8 0.9 copy-start
  51.4 13.4 %collective-permute-start.4 = (bf16[1536,128]{1,0:T(8,128)(2,1)}, bf16[1536,128]{1,0:T(8,128)(2,1)S(1)}, u32[]{:S(2)}, u32[]{:S(2)}) collective-permute-start(bf16[1536,128]{1,0:T(8,128)(2,1)} %get-tuple-element.26), channel_id=1, source_target_pairs={{0,16},{1,17},{2,18},{3,19},{4,20},{5,21},{6,22},{7,23},{8,24},{9,... | collective-permute-start | bytes 1179656 | tf_op jit(solution)/shard_map/ppermute | solution.py:295
  53.3 10.9 %collective-permute-start.5 = (f32[2,48,128]{2,1,0:T(8,128)S(1)}, f32[2,48,128]{2,1,0:T(8,128)S(1)}, u32[]{:S(2)}, u32[]{:S(2)}) collective-permute-start(f32[2,48,128]{2,1,0:T(8,128)S(1)} %add.16), channel_id=1, source_target_pairs={{0,16},{1,17},{2,18},{3,19},{4,20},{5,21},{6,22},{7,23},{8,24},{9,... | collective-permute-start | bytes 147464 | tf_op jit(solution)/shard_map/ppermute | solution.py:295
  64.8 0.7 copy-start.1
  103.9 8.5 %copy-start.2 = (bf16[8,192,128]{2,1,0:T(8,128)(2,1)}, bf16[8,192,128]{2,1,0:T(8,128)(2,1)S(1)}, u32[]{:S(2)}) copy-start(bf16[8,192,128]{2,1,0:T(8,128)(2,1)S(1)} %all_to_all.11) | copy-start | bytes 1179652
  103.9 12.8 %copy-start.6 = (bf16[3072]{0:T(1024)(128)(2,1)S(1)}, bf16[3072]{0:T(1024)(128)(2,1)}, u32[]{:S(2)}) copy-start(bf16[3072]{0:T(1024)(128)(2,1)} %param.25) | copy-start | bytes 18436
  103.9 8.5 %collective-permute-start.6 = (bf16[1536,128]{1,0:T(8,128)(2,1)S(1)}, bf16[1536,128]{1,0:T(8,128)(2,1)S(1)}, u32[]{:S(2)}, u32[]{:S(2)}) collective-permute-start(bf16[1536,128]{1,0:T(8,128)(2,1)S(1)} %bitcast.28), channel_id=1, source_target_pairs={{0,16},{1,17},{2,18},{3,19},{4,20},{5,21},{6,22},{7,23},{8,24},{9,... | collective-permute-start | bytes 1179656 | tf_op jit(solution)/shard_map/ppermute | solution.py:295
  112.4 0.8 copy-start.4
  116.7 8.1 %collective-permute-start.7 = (bf16[2,1536,128]{2,1,0:T(8,128)(2,1)}, bf16[2,1536,128]{2,1,0:T(8,128)(2,1)S(1)}, u32[]{:S(2)}, u32[]{:S(2)}) collective-permute-start(bf16[2,1536,128]{2,1,0:T(8,128)(2,1)} %get-tuple-element.28), channel_id=1, source_target_pairs={{0,8},{1,9},{2,10},{3,11},{4,12},{5,13},{6,14},{7,15},{8,0},{9,1},... | collective-permute-start | bytes 2359304 | tf_op jit(solution)/shard_map/ppermute | solution.py:295
  124.8 0.9 copy-start.3

commit v2 on v1

--- a/solution.py
+++ b/solution.py
@@ -27,14 +27,16 @@
     tri = iota((BLK, BLK), 0) - iota((BLK, BLK), 1)
 
     def one(raw, d, mask):
-        rate = jax.nn.softplus(raw + params[d : d + 1, :])
-        log = -jnp.exp(params[2 + d : 3 + d, :]) * rate + spread
-        cum = jnp.dot(mask.astype(f32), log, precision=HIGH, preferred_element_type=f32)
+        rate = jax.nn.softplus(raw + params[:, d : d + 1])
+        log = -jnp.exp(params[:, 2 + d : 3 + d]) * rate + spread
+        cum = jnp.dot(log, mask.astype(f32), precision=HIGH, preferred_element_type=f32)
         return rate, cum
 
-    rate_f, cum_f = one(ahead[0], 0, tri >= 0)
-    rate_b, cum_b = one(back[0], 1, tri <= 0)
-    tot_f, tot_b = cum_f[BLK - 1 :], cum_b[:1]
+    rate_f, cum_f = one(ahead[0], 0, tri <= 0)
+    rate_b, cum_b = one(back[0], 1, tri >= 0)
+    tot_f, tot_b = cum_f[:, BLK - 1 :], cum_b[:, :1]
+    totals[0] = jnp.broadcast_to(tot_f, totals.shape[1:])
+    totals[1] = jnp.broadcast_to(tot_b, totals.shape[1:])
     parts = (
         rate_f,
         rate_b,
@@ -45,25 +47,28 @@
         jnp.exp(cum_f),
         jnp.exp(cum_b),
     )
-    gap = jnp.zeros((BLK, SLOT - STEP_HEADS), f32)
-    rest = jnp.zeros((BLK, 128 - SLOT * len(parts)), f32)
+    gap = jnp.zeros((SLOT - STEP_HEADS, BLK), f32)
+    rest = jnp.zeros((128 - SLOT * len(parts), BLK), f32)
     for g in range(steps):
         at = slice(g * STEP_HEADS, (g + 1) * STEP_HEADS)
         pieces = []
         for part in parts:
-            pieces += [part[:, at], gap]
-        packed = jnp.concatenate(pieces + [rest], axis=1)
-        cols[g] = packed
-        turned = packed.T[: 4 * SLOT]
-        rows[g] = turned
-        for d, (start, end) in enumerate(((CF * SLOT, BLK - 1), (CB * SLOT, 0))):
-            last = turned[start : start + STEP_HEADS, end : end + 1]
-            totals[d, at] = jnp.broadcast_to(last, (STEP_HEADS, 128))
+            pieces += [part[at], gap]
+        packed = jnp.concatenate(pieces + [rest], axis=0)
+        rows[g] = packed[: 4 * SLOT]
+        cols[g] = packed.T
 
 
 def expand(cols, which, width):
-    pick = iota((128, width), 0) == which * SLOT + iota((128, width), 1) // HEAD_DIM
-    return jnp.dot(cols, pick.astype(f32), precision=HIGH, preferred_element_type=f32)
+    first = iota((BLK, 128), 1) < HEAD_DIM
+    start = which * SLOT
+    return jnp.concatenate(
+        [
+            jnp.where(first, cols[:, j : j + 1], cols[:, j + 1 : j + 2])
+            for j in range(start, start + width // HEAD_DIM, 2)
+        ],
+        axis=1,
+    )
 
 
 def conv(ref, halo, taps):
@@ -153,12 +158,18 @@
         ]
         y = y + jnp.where(first, by_group[0], by_group[1]) * expand(packed, which, width)
     gated = y.astype(bf16).astype(f32) * jax.nn.silu(gate[0].astype(f32))
-    same = iota((width, width), 0) // HEAD_DIM == iota((width, width), 1) // HEAD_DIM
-    mean = jnp.dot(
-        gated * gated,
-        jnp.where(same, 1.0 / HEAD_DIM, 0.0),
-        precision=HIGH,
-        preferred_element_type=f32,
+    same = iota((128, 128), 0) // HEAD_DIM == iota((128, 128), 1) // HEAD_DIM
+    ones = jnp.where(same, 1.0 / HEAD_DIM, 0.0).astype(bf16)
+    square = gated * gated
+    high = square.astype(bf16)
+    low = (square - high.astype(f32)).astype(bf16)
+    mean = jnp.concatenate(
+        [
+            jnp.dot(high[:, k : k + 128], ones, preferred_element_type=f32)
+            + jnp.dot(low[:, k : k + 128], ones, preferred_element_type=f32)
+            for k in range(0, width, 128)
+        ],
+        axis=1,
     )
     out[0] = (gated * lax.rsqrt(mean + 1e-6) * gain[...].astype(f32)).astype(bf16)
 
@@ -305,7 +316,7 @@
     )(place, *args)
 
 
-def exchange_tree(send, keep, logs, place):
+def exchange_tree(send, keep, logs, place, block):
     deep = lax.axis_size("dp")
     half = logs.shape[1] // 2
     whole_par = swap(logs, 1)
@@ -318,7 +329,7 @@
     theirs = swap(send, 1)
     rows = keep.shape[1:]
     across, stay = run(pair_kernel, (rows, rows), place, keep, theirs, own, par)
-    got = swap(across, 2)
+    y, got = lax.optimization_barrier((block(), swap(across, 2)))
     each = rows[0] // deep
     (packed,) = run(segment_kernel, ((deep, each + 16, STATE),), place, stay, got, pair, xpair)
     packed = lax.all_to_all(packed, "dp", split_axis=0, concat_axis=0)
@@ -328,7 +339,7 @@
     mine, back = run(
         enter_kernel, (keep.shape,) * 2, place, entry, other, got, keep, theirs, own, par, xpair
     )
-    return mine, swap(back, 1)
+    return mine, swap(back, 1), y
 
 
 def local(x, b, c, gate, ahead, back, fade, x_taps, b_taps, c_taps, offsets, exponents, gain):
@@ -357,10 +368,11 @@
     for piece in mine:
         bounds.append(bounds[-1] + piece.shape[1])
     gathered = lax.all_gather(jnp.concatenate(mine, axis=1), "sp")
-    xt, bt, ct, params = (
+    xt, bt, ct = (
         jnp.transpose(gathered[:, :, lo:hi], (1, 0, 2)).reshape(gathered.shape[1], -1)
-        for lo, hi in zip(bounds[:-1], bounds[1:])
-    )
+        for lo, hi in zip(bounds[:-2], bounds[1:-1])
+    )
+    params = jnp.transpose(gathered[:, :, bounds[-2] :], (0, 2, 1)).reshape(heads, -1)
     cols, rows, totals = pl.pallas_call(
         rates_kernel,
         out_shape=(
@@ -368,7 +380,7 @@
             jax.ShapeDtypeStruct((steps, 4 * SLOT, BLK), f32),
             jax.ShapeDtypeStruct((2, heads, 128), f32),
         ),
-    )(ahead, back, fade, params)
+    )(*(jnp.swapaxes(a, 1, 2) for a in (ahead, back, fade)), params)
 
     def raw(size):
         return pl.BlockSpec((1, tokens, size), lambda g: (0, 0, g))
@@ -443,7 +455,7 @@
             jax.ShapeDtypeStruct((2, x_width // 2, STATE), bf16),
         ],
     )(place, x, b, c, halo, halo, halo, xt, bt, ct, cols)
-    y = pl.pallas_call(
+    block = lambda: pl.pallas_call(
         block_kernel,
         grid=(steps,),
         in_specs=[
@@ -458,8 +470,9 @@
         compiler_params=params_,
     )(xc, bc, cc, cols, rows)
     if tree:
-        mine, theirs = exchange_tree(send, keep, totals, place)
+        mine, theirs, y = exchange_tree(send, keep, totals, place, block)
     else:
+        y = block()
         uf, ub = (jnp.concatenate([keep[d], send[d]], axis=0) for d in range(2))
         states = jnp.stack(exchange(uf, ub, totals[:, :, 0]))
         mine, theirs = states[:, : x_width // 2], states[:, x_width // 2 :]

time: 139 us -> 120 us (0.86)
  Pallas kernels: 48.5 us -> 39.6 us
  waiting for transfers between devices: 19.5 us -> 13.8 us
  local copies, waits for them, and re-layouts: 15.9 us -> 11.6 us
  blocking collectives: 42.8 us -> 41.4 us
    ppermute x6, waiting for transfers between devices: 19.5 us -> 13.8 us  [swap(): return lax.ppermute(a, ('sp', 'dp'), perm)]
    unnamed x17 -> x14, local copies, waits for them, and re-layouts: 7.69 us -> 3.27 us
    pallas_call x1, Pallas kernels: 14.9 us -> 10.9 us  [local(): half_call(state_kernel, [raw(xs), raw(bs), raw(bs), flat(16, xs), flat(16...]
    pallas_call x1, Pallas kernels: 12.3 us -> 8.94 us  [local(): half_call(finish_kernel, [flat(tokens, xs), flat(tokens, bs), stacked(BLK...]
    pallas_call x1, Pallas kernels: 3.68 us -> 2.18 us  [local(): pl.pallas_call(rates_kernel, out_shape=(jax.ShapeDtypeStruct((steps, BLK,...]
  transfers between devices with their start and end apart: 8 -> 8, of which waited for: 3 -> 4; matrix products, arithmetic and copies ran while one was open for 10% -> 9% of each run, Pallas kernels for 8% -> 8%
where the time goes in v2:
time: 120 us; the launch traced here: 118 us
  blocking collectives  41.4 us (34%)
  Pallas kernels  39.6 us (33%)
  waiting for transfers between devices  13.8 us (12%)
  local copies, waits for them, and re-layouts  11.6 us (10%)
  starting transfers between devices  7.47 us (6%)
  other arithmetic  4.27 us (4%)
    all_to_all x1, blocking collectives, exchange_tree(): packed = lax.all_to_all(packed, 'dp', split_axis=0, concat_axis=0)  18.1 us
    all_to_all x1, blocking collectives, exchange_tree(): lax.all_to_all(entry, 'dp', split_axis=0, concat_axis=0).reshape(rows)  15 us
    ppermute x6, waiting for transfers between devices, swap(): return lax.ppermute(a, ('sp', 'dp'), perm)  13.8 us
    pallas_call x1, Pallas kernels, local(): half_call(state_kernel, [raw(xs), raw(bs), raw(bs), flat(16, xs), flat(16...  10.9 us
    pallas_call x4, Pallas kernels, run(): pl.pallas_call(kernel, in_specs=[smem] + [vmem] * len(args), out_shape=[j...  10.1 us
    pallas_call x1, Pallas kernels, local(): half_call(finish_kernel, [flat(tokens, xs), flat(tokens, bs), stacked(BLK...  8.94 us
    all_gather x1, blocking collectives, local(): gathered = lax.all_gather(jnp.concatenate(mine, axis=1), 'sp')  8.29 us
    pallas_call x1, Pallas kernels, local(): pl.pallas_call(block_kernel, grid=(steps,), in_specs=[flat(tokens, xs), f...  7.48 us
  transfers between devices with their start and end apart: 8, of which 4 were waited for; matrix products, arithmetic and copies ran while one was open for 9% of the time, Pallas kernels for 8%

profile of v2, /device:TPU:0, one launch (start us, length us, event | category | flops | bytes accessed | tf_op | source)
XLA Modules:
  0.0 118.3 jit_solution(14856915553893532851)
XLA Ops:
  0.0 0.8 slice_bitcast_fusion
  0.8 0.8 slice_bitcast_fusion.3
  1.6 1.3 %collective-permute-start.1 = (bf16[1,7168]{1,0:T(2,128)(2,1)S(1)}, bf16[1,7168]{1,0:T(2,128)(2,1)S(1)}, u32[]{:S(2)}, u32[]{:S(2)}) collective-permute-start(bf16[1,7168]{1,0:T(2,128)(2,1)S(1)} %pad_maximum_fusion.1), channel_id=1, source_target_pairs={{8,0},{16,8},{24,16},{1,24},{9,1},{17,9},{25,17},{2,25},{10,2},{18... | collective-permute-start | bytes 43016 | tf_op jit(solution)/shard_map/ppermute | solution.py:360
  2.9 0.8 slice_bitcast_fusion.5
  3.7 0.8 slice_bitcast_fusion.1
  4.6 3.0 %collective-permute-start = (bf16[2,7168]{1,0:T(2,128)(2,1)S(1)}, bf16[2,7168]{1,0:T(2,128)(2,1)S(1)}, u32[]{:S(2)}, u32[]{:S(2)}) collective-permute-start(bf16[2,7168]{1,0:T(2,128)(2,1)S(1)} %pad_maximum_fusion), channel_id=1, source_target_pairs={{0,8},{8,16},{16,24},{24,1},{1,9},{9,17},{17,25},{25,2},{2,10},{10... | collective-permute-start | bytes 86024 | tf_op jit(solution)/shard_map/ppermute | solution.py:359
  7.7 0.7 convert_element_type.11
  9.0 0.7 convert_element_type.9
  9.7 0.7 maximum_bitcast_fusion
  10.4 8.3 %all-gather.1 = f32[4,4,1804]{2,1,0:T(4,128)S(1)} all-gather(f32[1,4,1804]{2,1,0:T(4,128)S(1)} %maximum_bitcast_fusion), channel_id=2, replica_groups=mesh['sp'=4,'dp'=8] {'sp'}, dimensions={0}, use_global_device_ids=true | all-gather | bytes 144320 | tf_op jit(solution)/shard_map/all_gather | solution.py:370
  20.8 0.7 copy.18.params
  21.5 2.2 %shard_map.127 = (f32[8,128,128]{2,1,0:T(8,128)}, f32[8,32,128]{2,1,0:T(8,128)}, f32[2,48,128]{2,1,0:T(8,128)}) custom-call(f32[1,48,128]{2,1,0:T(8,128)} %bitcast.38, f32[1,48,128]{2,1,0:T(8,128)} %bitcast.39, f32[1,48,128]{2,1,0:T(8,128)} %bitcast.40, f32[48,4]{1,0:T(8,128)} %copy.18.params), custom_call_target="tpu_custom_call" | custom-call | tf_op jit(solution)/shard_map/pallas_call | solution.py:376
  23.6 0.8 maximum_maximum_fusion.xh.bh.ch
  24.5 10.9 %shard_map.128 = (bf16[128,3072]{1,0:T(8,128)(2,1)}, bf16[128,2048]{1,0:T(8,128)(2,1)}, bf16[128,2048]{1,0:T(8,128)(2,1)}, bf16[2,1536,128]{2,1,0:T(8,128)(2,1)}, bf16[2,1536,128]{2,1,0:T(8,128)(2,1)}) custom-call(s32[2]{0:T(128)} %pad_add_fusion.place, bf16[1,128,3072]{2,1,0:T(8,128)(2,1)} %x.1, bf16[1,128,2048]{2,1,0:T(8,128)(2,1)} %b.1, ...), custom_call_target="tpu_custom_call" | custom-call | tf_op jit(solution)/shard_map/pallas_call | solution.py:432
  36.5 1.5 %collective-permute-done.3 = f32[2,48,128]{2,1,0:T(8,128)S(1)} collective-permute-done((f32[2,48,128]{2,1,0:T(8,128)S(1)}, f32[2,48,128]{2,1,0:T(8,128)S(1)}, u32[]{:S(2)}, u32[]{:S(2)}) %collective-permute-start.3) | collective-permute-done | bytes 49184 | tf_op jit(solution)/shard_map/ppermute | solution.py:306
  38.6 0.9 copy-done
  39.4 2.6 %shard_map.130 = (bf16[1536,128]{1,0:T(8,128)(2,1)}, bf16[1536,128]{1,0:T(8,128)(2,1)}) custom-call(s32[2]{0:T(128)} %pad_add_fusion.place, bf16[2,1536,128]{2,1,0:T(8,128)(2,1)} %get-tuple-element.24.mine, bf16[2,1536,128]{2,1,0:T(8,128)(2,1)} %copy-done, f32[2,24,128]{2,1,0:T(8,128)} %constant_dynamic-slice_fusion.3.own, ...), custom_call_target="tpu_custom_call" | custom-call | tf_op jit(solution)/shard_map/pallas_call | solution.py:312
  42.1 0.7 collective-permute-start.4
  42.8 7.5 %shard_map.129.local = f32[128,3072]{1,0:T(8,128)} custom-call(bf16[128,3072]{1,0:T(8,128)(2,1)} %get-tuple-element.20.x, bf16[128,2048]{1,0:T(8,128)(2,1)} %get-tuple-element.21.b, bf16[128,2048]{1,0:T(8,128)(2,1)} %get-tuple-element.22.c, f32[8,128,128]{2,1,0:T(8,128)} %get-tuple-element.19.cols, f32[8,32,128]{2,1,0:T(8,128)} %get-tuple-element.23.rows), custom_call_target="tpu_custom_call" | custom-call | tf_op jit(solution)/shard_map/pallas_call | solution.py:458
  50.3 1.4 %collective-permute-start.5 = (f32[2,48,128]{2,1,0:T(8,128)S(1)}, f32[2,48,128]{2,1,0:T(8,128)S(1)}, u32[]{:S(2)}, u32[]{:S(2)}) collective-permute-start(f32[2,48,128]{2,1,0:T(8,128)S(1)} %add.16), channel_id=1, source_target_pairs={{0,16},{1,17},{2,18},{3,19},{4,20},{5,21},{6,22},{7,23},{8,24},{9,... | collective-permute-start | bytes 147464 | tf_op jit(solution)/shard_map/ppermute | solution.py:306
  52.3 2.4 %collective-permute-done.5 = f32[2,48,128]{2,1,0:T(8,128)S(1)} collective-permute-done((f32[2,48,128]{2,1,0:T(8,128)S(1)}, f32[2,48,128]{2,1,0:T(8,128)S(1)}, u32[]{:S(2)}, u32[]{:S(2)}) %collective-permute-start.5) | collective-permute-done | bytes 49184 | tf_op jit(solution)/shard_map/ppermute | solution.py:306
  55.3 0.8 copy-done.1
  56.1 2.0 %shard_map.131 = bf16[8,208,128]{2,1,0:T(8,128)(2,1)} custom-call(s32[2]{0:T(128)} %pad_add_fusion.place, bf16[1536,128]{1,0:T(8,128)(2,1)} %get-tuple-element.29.keep, bf16[1536,128]{1,0:T(8,128)(2,1)} %copy-done.1, f32[2,24,128]{2,1,0:T(8,128)} %constant_dynamic-slice_fusion.1.pair, f32[2,24,128]{2,1,0:T(8,128)} %constant_dynamic-slice_fusion.xpair), custom_call_target="tpu_custom_call" | custom-call | tf_op jit(solution)/shard_map/pallas_call | solution.py:312
  58.1 18.1 %all_to_all.10.v = bf16[8,208,128]{2,1,0:T(8,128)(2,1)} all-to-all(bf16[8,208,128]{2,1,0:T(8,128)(2,1)} %shard_map.131), channel_id=1, replica_groups=mesh['sp'=4,'dp'=8] {'dp'}, dimensions={0} | all-to-all | bytes 851968 | tf_op jit(solution)/shard_map/all_to_all | solution.py:335
  76.3 1.9 %shard_map.132 = bf16[8,192,128]{2,1,0:T(8,128)(2,1)} custom-call(s32[2]{0:T(128)} %pad_add_fusion.place, bf16[8,208,128]{2,1,0:T(8,128)(2,1)} %all_to_all.10.v), custom_call_target="tpu_custom_call" | custom-call | tf_op jit(solution)/shard_map/pallas_call | solution.py:312
  78.1 15.0 %all_to_all.11 = bf16[8,192,128]{2,1,0:T(8,128)(2,1)S(1)} all-to-all(bf16[8,192,128]{2,1,0:T(8,128)(2,1)} %shard_map.132), channel_id=1, replica_groups=mesh['sp'=4,'dp'=8] {'dp'}, dimensions={0} | all-to-all | bytes 786432 | tf_op jit(solution)/shard_map/all_to_all | solution.py:337
  93.6 8.0 %collective-permute-done.6.other = bf16[1536,128]{1,0:T(8,128)(2,1)S(1)} collective-permute-done((bf16[1536,128]{1,0:T(8,128)(2,1)S(1)}, bf16[1536,128]{1,0:T(8,128)(2,1)S(1)}, u32[]{:S(2)}, u32[]{:S(2)}) %collective-permute-start.6) | collective-permute-done | bytes 393248 | tf_op jit(solution)/shard_map/ppermute | solution.py:306
  101.7 0.7 copy-done.4
  102.4 3.6 %shard_map.133 = (bf16[2,1536,128]{2,1,0:T(8,128)(2,1)}, bf16[2,1536,128]{2,1,0:T(8,128)(2,1)}) custom-call(s32[2]{0:T(128)} %pad_add_fusion.place, bf16[1536,128]{1,0:T(8,128)(2,1)} %bitcast.34, bf16[1536,128]{1,0:T(8,128)(2,1)} %copy-done.4, bf16[1536,128]{1,0:T(8,128)(2,1)} %copy-done.1, bf16[2,1536,128]{2,1,0:T(8,128)(2,1)} %get-tuple-element.24.mine, ...), custom_call_target="tpu_custom_call" | custom-call | tf_op jit(solution)/shard_map/pallas_call | solution.py:312
  106.6 1.9 %collective-permute-done.7.theirs = bf16[2,1536,128]{2,1,0:T(8,128)(2,1)S(1)} collective-permute-done((bf16[2,1536,128]{2,1,0:T(8,128)(2,1)}, bf16[2,1536,128]{2,1,0:T(8,128)(2,1)S(1)}, u32[]{:S(2)}, u32[]{:S(2)}) %collective-permute-start.7) | collective-permute-done | bytes 786464 | tf_op jit(solution)/shard_map/ppermute | solution.py:306
  108.5 0.9 copy-done.3
  109.3 8.9 %shard_map.134 = bf16[1,128,3072]{2,1,0:T(8,128)(2,1)} custom-call(s32[2]{0:T(128)} %pad_add_fusion.place, f32[128,3072]{1,0:T(8,128)} %shard_map.129.local, bf16[128,2048]{1,0:T(8,128)(2,1)} %get-tuple-element.22.c, f32[8,128,128]{2,1,0:T(8,128)} %get-tuple-element.19.cols, bf16[2,1536,128]{2,1,0:T(8,128)(2,1)} %get-tuple-element.31.mine, ...), custom_call_target="tpu_custom_call" | custom-call | tf_op jit(solution)/shard_map/pallas_call | solution.py:479
  (37 shorter events, 6.9 us)
Async XLA Ops:
  1.6 22.0 %collective-permute-start.1 = (bf16[1,7168]{1,0:T(2,128)(2,1)S(1)}, bf16[1,7168]{1,0:T(2,128)(2,1)S(1)}, u32[]{:S(2)}, u32[]{:S(2)}) collective-permute-start(bf16[1,7168]{1,0:T(2,128)(2,1)S(1)} %pad_maximum_fusion.1), channel_id=1, source_target_pairs={{8,0},{16,8},{24,16},{1,24},{9,1},{17,9},{25,17},{2,25},{10,2},{18... | collective-permute-start | bytes 43016 | tf_op jit(solution)/shard_map/ppermute | solution.py:360
  4.6 19.0 %collective-permute-start = (bf16[2,7168]{1,0:T(2,128)(2,1)S(1)}, bf16[2,7168]{1,0:T(2,128)(2,1)S(1)}, u32[]{:S(2)}, u32[]{:S(2)}) collective-permute-start(bf16[2,7168]{1,0:T(2,128)(2,1)S(1)} %pad_maximum_fusion), channel_id=1, source_target_pairs={{0,8},{8,16},{16,24},{24,1},{1,9},{9,17},{17,25},{25,2},{2,10},{10... | collective-permute-start | bytes 86024 | tf_op jit(solution)/shard_map/ppermute | solution.py:359
  24.5 11.3 %copy-start.5 = (f32[2,48,128]{2,1,0:T(8,128)S(1)}, f32[2,48,128]{2,1,0:T(8,128)}, u32[]{:S(2)}) copy-start(f32[2,48,128]{2,1,0:T(8,128)} %get-tuple-element.26) | copy-start | bytes 147460
  35.3 3.2 %collective-permute-start.2 = (bf16[2,1536,128]{2,1,0:T(8,128)(2,1)}, bf16[2,1536,128]{2,1,0:T(8,128)(2,1)S(1)}, u32[]{:S(2)}, u32[]{:S(2)}) collective-permute-start(bf16[2,1536,128]{2,1,0:T(8,128)(2,1)} %get-tuple-element.25), channel_id=1, source_target_pairs={{0,8},{1,9},{2,10},{3,11},{4,12},{5,13},{6,14},{7,15},{8,0},{9,1},... | collective-permute-start | bytes 2359304 | tf_op jit(solution)/shard_map/ppermute | solution.py:306
  35.7 2.2 %collective-permute-start.3 = (f32[2,48,128]{2,1,0:T(8,128)S(1)}, f32[2,48,128]{2,1,0:T(8,128)S(1)}, u32[]{:S(2)}, u32[]{:S(2)}) collective-permute-start(f32[2,48,128]{2,1,0:T(8,128)S(1)} %copy-done.5), channel_id=1, source_target_pairs={{0,8},{1,9},{2,10},{3,11},{4,12},{5,13},{6,14},{7,15},{8,0},{9,1},... | collective-permute-start | bytes 147464 | tf_op jit(solution)/shard_map/ppermute | solution.py:306
  38.6 0.9 copy-start
  42.1 13.2 %collective-permute-start.4 = (bf16[1536,128]{1,0:T(8,128)(2,1)}, bf16[1536,128]{1,0:T(8,128)(2,1)S(1)}, u32[]{:S(2)}, u32[]{:S(2)}) collective-permute-start(bf16[1536,128]{1,0:T(8,128)(2,1)} %get-tuple-element.27), channel_id=1, source_target_pairs={{0,16},{1,17},{2,18},{3,19},{4,20},{5,21},{6,22},{7,23},{8,24},{9,... | collective-permute-start | bytes 1179656 | tf_op jit(solution)/shard_map/ppermute | solution.py:306
  50.3 4.4 %collective-permute-start.5 = (f32[2,48,128]{2,1,0:T(8,128)S(1)}, f32[2,48,128]{2,1,0:T(8,128)S(1)}, u32[]{:S(2)}, u32[]{:S(2)}) collective-permute-start(f32[2,48,128]{2,1,0:T(8,128)S(1)} %add.16), channel_id=1, source_target_pairs={{0,16},{1,17},{2,18},{3,19},{4,20},{5,21},{6,22},{7,23},{8,24},{9,... | collective-permute-start | bytes 147464 | tf_op jit(solution)/shard_map/ppermute | solution.py:306
  55.3 0.8 copy-start.1
  93.1 8.5 %copy-start.2 = (bf16[8,192,128]{2,1,0:T(8,128)(2,1)}, bf16[8,192,128]{2,1,0:T(8,128)(2,1)S(1)}, u32[]{:S(2)}) copy-start(bf16[8,192,128]{2,1,0:T(8,128)(2,1)S(1)} %all_to_all.11) | copy-start | bytes 1179652
  93.1 12.8 %copy-start.6 = (bf16[3072]{0:T(1024)(128)(2,1)S(1)}, bf16[3072]{0:T(1024)(128)(2,1)}, u32[]{:S(2)}) copy-start(bf16[3072]{0:T(1024)(128)(2,1)} %param.25) | copy-start | bytes 18436
  93.1 8.5 %collective-permute-start.6 = (bf16[1536,128]{1,0:T(8,128)(2,1)S(1)}, bf16[1536,128]{1,0:T(8,128)(2,1)S(1)}, u32[]{:S(2)}, u32[]{:S(2)}) collective-permute-start(bf16[1536,128]{1,0:T(8,128)(2,1)S(1)} %bitcast.33), channel_id=1, source_target_pairs={{0,16},{1,17},{2,18},{3,19},{4,20},{5,21},{6,22},{7,23},{8,24},{9,... | collective-permute-start | bytes 1179656 | tf_op jit(solution)/shard_map/ppermute | solution.py:306
  101.7 0.7 copy-start.4
  106.0 2.5 %collective-permute-start.7 = (bf16[2,1536,128]{2,1,0:T(8,128)(2,1)}, bf16[2,1536,128]{2,1,0:T(8,128)(2,1)S(1)}, u32[]{:S(2)}, u32[]{:S(2)}) collective-permute-start(bf16[2,1536,128]{2,1,0:T(8,128)(2,1)} %get-tuple-element.32), channel_id=1, source_target_pairs={{0,8},{1,9},{2,10},{3,11},{4,12},{5,13},{6,14},{7,15},{8,0},{9,1},... | collective-permute-start | bytes 2359304 | tf_op jit(solution)/shard_map/ppermute | solution.py:306
  108.5 0.9 copy-start.3

commit v3 on v2

--- a/solution.py
+++ b/solution.py
@@ -19,6 +19,22 @@
 
 def iota(shape, dim):
     return lax.broadcasted_iota(jnp.int32, shape, dim)
+
+
+def edge_kernel(xl, bl, cl, xf, bf, cf, xt, bt, ct, offsets, exponents, low, high, packed):
+    at = 0
+    for end, start in ((xl, xf), (bl, bf), (cl, cf)):
+        to = at + end.shape[2]
+        rows = end.shape[1]
+        low[:, at:to] = end[0].astype(f32)[rows - 2 :].astype(bf16)
+        high[:, at:to] = start[0].astype(f32)[:1].astype(bf16)
+        at = to
+    at = 0
+    for part in (xt, bt, ct):
+        packed[:, at : at + part.shape[1]] = part[...].astype(f32)
+        at += part.shape[1]
+    packed[0:2, at:] = offsets[...]
+    packed[2:4, at:] = exponents[...]
 
 
 def rates_kernel(ahead, back, fade, params, cols, rows, totals):
@@ -353,21 +369,41 @@
     up = list(zip(order[:-1], order[1:]))
     down = [(target, source) for source, target in up]
 
-    def edge(rows):
-        return jnp.concatenate([x[0, rows], b[0, rows], c[0, rows]], axis=1)
-
-    low = lax.ppermute(edge(slice(tokens - 2, tokens)), ("sp", "dp"), up)
-    high = lax.ppermute(edge(slice(0, 1)), ("sp", "dp"), down)
+    bounds = [0]
+    for piece in (x_taps, b_taps, c_taps, offsets):
+        bounds.append(bounds[-1] + piece.shape[1])
+    rows_at = [(1, 16, a.shape[2]) for a in (x, b, c)]
+    final = tokens // 16 - 1
+    small = (x_taps, b_taps, c_taps, offsets, exponents)
+    low, high, mine = pl.pallas_call(
+        edge_kernel,
+        grid=(1,),
+        in_specs=[pl.BlockSpec(shape, lambda i: (0, final, 0)) for shape in rows_at]
+        + [pl.BlockSpec(shape, lambda i: (0, 0, 0)) for shape in rows_at]
+        + [pl.BlockSpec(a.shape, lambda i: (0, 0)) for a in small],
+        out_shape=[
+            jax.ShapeDtypeStruct((2, x_width + 2 * b_width), bf16),
+            jax.ShapeDtypeStruct((1, x_width + 2 * b_width), bf16),
+            jax.ShapeDtypeStruct((x_taps.shape[0], bounds[-1]), f32),
+        ],
+    )(x, b, c, x, b, c, *small)
+    if wide == 4:
+        spot = lax.axis_index("sp")
+        even, left = spot % 2 == 0, spot < 2
+        sent = [swap(mine, bit) for bit in (1, 2, 3)]
+        near = [jnp.where(even, mine, sent[0]), jnp.where(even, sent[0], mine)]
+        far = [jnp.where(even, sent[1], sent[2]), jnp.where(even, sent[2], sent[1])]
+        gathered = jnp.stack(
+            [jnp.where(left, u, v) for u, v in zip(near + far, far + near)]
+        )
+    else:
+        gathered = lax.all_gather(mine, "sp")
+    low = lax.ppermute(low, ("sp", "dp"), up)
+    high = lax.ppermute(high, ("sp", "dp"), down)
     width = low.shape[1]
     halo = jnp.concatenate(
         [jnp.zeros((6, width), bf16), low, high, jnp.zeros((7, width), bf16)], axis=0
     )
-    mine = [t.astype(f32) for t in (x_taps, b_taps, c_taps)]
-    mine.append(jnp.concatenate([offsets, exponents], axis=0))
-    bounds = [0]
-    for piece in mine:
-        bounds.append(bounds[-1] + piece.shape[1])
-    gathered = lax.all_gather(jnp.concatenate(mine, axis=1), "sp")
     xt, bt, ct = (
         jnp.transpose(gathered[:, :, lo:hi], (1, 0, 2)).reshape(gathered.shape[1], -1)
         for lo, hi in zip(bounds[:-2], bounds[1:-1])

time: 120 us -> 116 us (0.967)
  blocking collectives: 41.4 us -> 35.2 us
  starting transfers between devices: 7.47 us -> 12.6 us
  local copies, waits for them, and re-layouts: 11.6 us -> 8.49 us
  other arithmetic: 4.27 us -> 2.28 us
  Pallas kernels: 39.6 us -> 41.3 us
    all_gather x1 -> x0, blocking collectives: 8.29 us -> none  [local(): gathered = lax.all_gather(jnp.concatenate(mine, axis=1), 'sp')]
    ppermute x6 -> x9, starting transfers between devices: 3.15 us -> 8.33 us  [swap(): return lax.ppermute(a, ('sp', 'dp'), perm)]
    squeeze x4 -> x0, local copies, waits for them, and re-layouts: 3.21 us -> none  [edge(): return jnp.concatenate([x[0, rows], b[0, rows], c[0, rows]], axis=1)]
    convert_element_type x3 -> x0, other arithmetic: 2.08 us -> none  [local(): mine = [t.astype(f32) for t in (x_taps, b_taps, c_taps)]]
    all_to_all x1, blocking collectives: 18.1 us -> 20.2 us  [exchange_tree(): packed = lax.all_to_all(packed, 'dp', split_axis=0, concat_axis=0)]
    pallas_call x0 -> x1, Pallas kernels: none -> 1.73 us  [local(): pl.pallas_call(edge_kernel, grid=(1,), in_specs=[pl.BlockSpec(shape, lamb...]
    ppermute x6 -> x9, waiting for transfers between devices: 13.8 us -> 14.7 us  [swap(): return lax.ppermute(a, ('sp', 'dp'), perm)]
  transfers between devices with their start and end apart: 8 -> 11, of which waited for: 4 -> 5; matrix products, arithmetic and copies ran while one was open for 9% -> 4% of each run, Pallas kernels for 8% -> 6%
where the time goes in v3:
time: 116 us; the launch traced here: 115 us
  Pallas kernels  41.3 us (36%)
  blocking collectives  35.2 us (30%)
  waiting for transfers between devices  15 us (13%)
  starting transfers between devices  12.6 us (11%)
  local copies, waits for them, and re-layouts  8.49 us (7%)
  other arithmetic  2.28 us (2%)
    all_to_all x1, blocking collectives, exchange_tree(): packed = lax.all_to_all(packed, 'dp', split_axis=0, concat_axis=0)  20.2 us
    all_to_all x1, blocking collectives, exchange_tree(): lax.all_to_all(entry, 'dp', split_axis=0, concat_axis=0).reshape(rows)  15 us
    ppermute x9, waiting for transfers between devices, swap(): return lax.ppermute(a, ('sp', 'dp'), perm)  14.7 us
    pallas_call x1, Pallas kernels, local(): half_call(state_kernel, [raw(xs), raw(bs), raw(bs), flat(16, xs), flat(16...  10.9 us
    pallas_call x4, Pallas kernels, run(): pl.pallas_call(kernel, in_specs=[smem] + [vmem] * len(args), out_shape=[j...  10.1 us
    pallas_call x1, Pallas kernels, local(): half_call(finish_kernel, [flat(tokens, xs), flat(tokens, bs), stacked(BLK...  8.94 us
    ppermute x9, starting transfers between devices, swap(): return lax.ppermute(a, ('sp', 'dp'), perm)  8.33 us
    pallas_call x1, Pallas kernels, local(): pl.pallas_call(block_kernel, grid=(steps,), in_specs=[flat(tokens, xs), f...  7.45 us
  transfers between devices with their start and end apart: 11, of which 5 were waited for; matrix products, arithmetic and copies ran while one was open for 4% of the time, Pallas kernels for 6%

profile of v3, /device:TPU:0, one launch (start us, length us, event | category | flops | bytes accessed | tf_op | source)
XLA Modules:
  0.0 115.0 jit_solution(10544608992436570645)
XLA Ops:
  0.0 1.7 %shard_map.127 = (bf16[2,7168]{1,0:T(2,128)(2,1)}, bf16[1,7168]{1,0:T(2,128)(2,1)}, f32[4,1804]{1,0:T(4,128)}) custom-call(bf16[1,128,3072]{2,1,0:T(8,128)(2,1)} %x.1, bf16[1,128,2048]{2,1,0:T(8,128)(2,1)} %b.1, bf16[1,128,2048]{2,1,0:T(8,128)(2,1)} %c.1, bf16[1,128,3072]{2,1,0:T(8,128)(2,1)} %x.1, bf16[1,128,2048]{2,1,0:T(8,128)(2,1)} %b.1, ...), custom_call_target="tpu_custom_call" | custom-call | tf_op jit(solution)/shard_map/pallas_call | solution.py:378
  2.2 2.5 %collective-permute-start.3 = (f32[4,1804]{1,0:T(4,128)}, f32[4,1804]{1,0:T(4,128)S(1)}, u32[]{:S(2)}, u32[]{:S(2)}) collective-permute-start(f32[4,1804]{1,0:T(4,128)} %get-tuple-element.24), channel_id=1, source_target_pairs={{0,16},{1,17},{2,18},{3,19},{4,20},{5,21},{6,22},{7,23},{8,24},{9,... | collective-permute-start | bytes 86600 | tf_op jit(solution)/shard_map/ppermute | solution.py:322
  4.8 1.3 %collective-permute-start.1 = (bf16[1,7168]{1,0:T(2,128)(2,1)}, bf16[1,7168]{1,0:T(2,128)(2,1)S(1)}, u32[]{:S(2)}, u32[]{:S(2)}) collective-permute-start(bf16[1,7168]{1,0:T(2,128)(2,1)} %get-tuple-element.23), channel_id=1, source_target_pairs={{8,0},{16,8},{24,16},{1,24},{9,1},{17,9},{25,17},{2,25},{10,2},{18... | collective-permute-start | bytes 43016 | tf_op jit(solution)/shard_map/ppermute | solution.py:402
  6.1 3.0 %collective-permute-start = (bf16[2,7168]{1,0:T(2,128)(2,1)}, bf16[2,7168]{1,0:T(2,128)(2,1)S(1)}, u32[]{:S(2)}, u32[]{:S(2)}) collective-permute-start(bf16[2,7168]{1,0:T(2,128)(2,1)} %get-tuple-element.22), channel_id=1, source_target_pairs={{0,8},{8,16},{16,24},{24,1},{1,9},{9,17},{17,25},{25,2},{2,10},{10... | collective-permute-start | bytes 86024 | tf_op jit(solution)/shard_map/ppermute | solution.py:401
  9.2 0.7 pad_add_fusion.place
  10.2 0.8 maximum_maximum_fusion.xh.bh.ch
  11.0 0.8 select_bitcast_fusion.3
  11.8 0.6 slice.16
  12.4 0.6 fusion
  13.2 0.7 copy.16.params
  13.9 2.2 %shard_map.128 = (f32[8,128,128]{2,1,0:T(8,128)}, f32[8,32,128]{2,1,0:T(8,128)}, f32[2,48,128]{2,1,0:T(8,128)}) custom-call(f32[1,48,128]{2,1,0:T(8,128)} %bitcast.32, f32[1,48,128]{2,1,0:T(8,128)} %bitcast.33, f32[1,48,128]{2,1,0:T(8,128)} %bitcast.34, f32[48,4]{1,0:T(8,128)} %copy.16.params), custom_call_target="tpu_custom_call" | custom-call | tf_op jit(solution)/shard_map/pallas_call | solution.py:412
  16.1 10.9 %shard_map.129 = (bf16[128,3072]{1,0:T(8,128)(2,1)}, bf16[128,2048]{1,0:T(8,128)(2,1)}, bf16[128,2048]{1,0:T(8,128)(2,1)}, bf16[2,1536,128]{2,1,0:T(8,128)(2,1)}, bf16[2,1536,128]{2,1,0:T(8,128)(2,1)}) custom-call(s32[2]{0:T(128)} %pad_add_fusion.place, bf16[1,128,3072]{2,1,0:T(8,128)(2,1)} %x.1, bf16[1,128,2048]{2,1,0:T(8,128)(2,1)} %b.1, ...), custom_call_target="tpu_custom_call" | custom-call | tf_op jit(solution)/shard_map/pallas_call | solution.py:468
  26.9 1.6 %collective-permute-start.5 = (bf16[2,1536,128]{2,1,0:T(8,128)(2,1)}, bf16[2,1536,128]{2,1,0:T(8,128)(2,1)S(1)}, u32[]{:S(2)}, u32[]{:S(2)}) collective-permute-start(bf16[2,1536,128]{2,1,0:T(8,128)(2,1)} %get-tuple-element.31), channel_id=1, source_target_pairs={{0,8},{1,9},{2,10},{3,11},{4,12},{5,13},{6,14},{7,15},{8,0},{9,1},... | collective-permute-start | bytes 2359304 | tf_op jit(solution)/shard_map/ppermute | solution.py:322
  29.2 1.5 %collective-permute-done.6 = f32[2,48,128]{2,1,0:T(8,128)S(1)} collective-permute-done((f32[2,48,128]{2,1,0:T(8,128)S(1)}, f32[2,48,128]{2,1,0:T(8,128)S(1)}, u32[]{:S(2)}, u32[]{:S(2)}) %collective-permute-start.6) | collective-permute-done | bytes 49184 | tf_op jit(solution)/shard_map/ppermute | solution.py:322
  31.3 0.9 copy-done
  32.2 2.7 %shard_map.131 = (bf16[1536,128]{1,0:T(8,128)(2,1)}, bf16[1536,128]{1,0:T(8,128)(2,1)}) custom-call(s32[2]{0:T(128)} %pad_add_fusion.place, bf16[2,1536,128]{2,1,0:T(8,128)(2,1)} %get-tuple-element.30.mine, bf16[2,1536,128]{2,1,0:T(8,128)(2,1)} %copy-done, f32[2,24,128]{2,1,0:T(8,128)} %constant_dynamic-slice_fusion.3.own, ...), custom_call_target="tpu_custom_call" | custom-call | tf_op jit(solution)/shard_map/pallas_call | solution.py:328
  34.9 2.9 %collective-permute-start.7 = (bf16[1536,128]{1,0:T(8,128)(2,1)}, bf16[1536,128]{1,0:T(8,128)(2,1)S(1)}, u32[]{:S(2)}, u32[]{:S(2)}) collective-permute-start(bf16[1536,128]{1,0:T(8,128)(2,1)} %get-tuple-element.33), channel_id=1, source_target_pairs={{0,16},{1,17},{2,18},{3,19},{4,20},{5,21},{6,22},{7,23},{8,24},{9,... | collective-permute-start | bytes 1179656 | tf_op jit(solution)/shard_map/ppermute | solution.py:322
  37.7 7.5 %shard_map.130.local = f32[128,3072]{1,0:T(8,128)} custom-call(bf16[128,3072]{1,0:T(8,128)(2,1)} %get-tuple-element.26.x, bf16[128,2048]{1,0:T(8,128)(2,1)} %get-tuple-element.27.b, bf16[128,2048]{1,0:T(8,128)(2,1)} %get-tuple-element.28.c, f32[8,128,128]{2,1,0:T(8,128)} %get-tuple-element.25.cols, f32[8,32,128]{2,1,0:T(8,128)} %get-tuple-element.29.rows), custom_call_target="tpu_custom_call" | custom-call | tf_op jit(solution)/shard_map/pallas_call | solution.py:494
  45.3 0.6 constant_dynamic-slice_fusion.1.pair
  45.9 3.5 %collective-permute-done.8 = f32[2,48,128]{2,1,0:T(8,128)S(1)} collective-permute-done((f32[2,48,128]{2,1,0:T(8,128)S(1)}, f32[2,48,128]{2,1,0:T(8,128)S(1)}, u32[]{:S(2)}, u32[]{:S(2)}) %collective-permute-start.8) | collective-permute-done | bytes 49184 | tf_op jit(solution)/shard_map/ppermute | solution.py:322
  50.0 0.8 copy-done.1
  50.7 2.0 %shard_map.132 = bf16[8,208,128]{2,1,0:T(8,128)(2,1)} custom-call(s32[2]{0:T(128)} %pad_add_fusion.place, bf16[1536,128]{1,0:T(8,128)(2,1)} %get-tuple-element.35.keep, bf16[1536,128]{1,0:T(8,128)(2,1)} %copy-done.1, f32[2,24,128]{2,1,0:T(8,128)} %constant_dynamic-slice_fusion.1.pair, f32[2,24,128]{2,1,0:T(8,128)} %constant_dynamic-slice_fusion.xpair), custom_call_target="tpu_custom_call" | custom-call | tf_op jit(solution)/shard_map/pallas_call | solution.py:328
  52.8 20.2 %all_to_all.10.v = bf16[8,208,128]{2,1,0:T(8,128)(2,1)} all-to-all(bf16[8,208,128]{2,1,0:T(8,128)(2,1)} %shard_map.132), channel_id=1, replica_groups=mesh['sp'=4,'dp'=8] {'dp'}, dimensions={0} | all-to-all | bytes 851968 | tf_op jit(solution)/shard_map/all_to_all | solution.py:351
  72.9 1.9 %shard_map.133 = bf16[8,192,128]{2,1,0:T(8,128)(2,1)} custom-call(s32[2]{0:T(128)} %pad_add_fusion.place, bf16[8,208,128]{2,1,0:T(8,128)(2,1)} %all_to_all.10.v), custom_call_target="tpu_custom_call" | custom-call | tf_op jit(solution)/shard_map/pallas_call | solution.py:328
  74.8 15.0 %all_to_all.11 = bf16[8,192,128]{2,1,0:T(8,128)(2,1)S(1)} all-to-all(bf16[8,192,128]{2,1,0:T(8,128)(2,1)} %shard_map.133), channel_id=1, replica_groups=mesh['sp'=4,'dp'=8] {'dp'}, dimensions={0} | all-to-all | bytes 786432 | tf_op jit(solution)/shard_map/all_to_all | solution.py:353
  89.8 0.7 collective-permute-start.9
  90.5 7.9 %collective-permute-done.9.other = bf16[1536,128]{1,0:T(8,128)(2,1)S(1)} collective-permute-done((bf16[1536,128]{1,0:T(8,128)(2,1)S(1)}, bf16[1536,128]{1,0:T(8,128)(2,1)S(1)}, u32[]{:S(2)}, u32[]{:S(2)}) %collective-permute-start.9) | collective-permute-done | bytes 393248 | tf_op jit(solution)/shard_map/ppermute | solution.py:322
  98.3 0.8 copy-done.4
  99.1 3.6 %shard_map.134 = (bf16[2,1536,128]{2,1,0:T(8,128)(2,1)}, bf16[2,1536,128]{2,1,0:T(8,128)(2,1)}) custom-call(s32[2]{0:T(128)} %pad_add_fusion.place, bf16[1536,128]{1,0:T(8,128)(2,1)} %bitcast.28, bf16[1536,128]{1,0:T(8,128)(2,1)} %copy-done.4, bf16[1536,128]{1,0:T(8,128)(2,1)} %copy-done.1, bf16[2,1536,128]{2,1,0:T(8,128)(2,1)} %get-tuple-element.30.mine, ...), custom_call_target="tpu_custom_call" | custom-call | tf_op jit(solution)/shard_map/pallas_call | solution.py:328
  103.3 1.9 %collective-permute-done.10.theirs = bf16[2,1536,128]{2,1,0:T(8,128)(2,1)S(1)} collective-permute-done((bf16[2,1536,128]{2,1,0:T(8,128)(2,1)}, bf16[2,1536,128]{2,1,0:T(8,128)(2,1)S(1)}, u32[]{:S(2)}, u32[]{:S(2)}) %collective-permute-start.10) | collective-permute-done | bytes 786464 | tf_op jit(solution)/shard_map/ppermute | solution.py:322
  105.2 0.9 copy-done.3
  106.0 8.9 %shard_map.135 = bf16[1,128,3072]{2,1,0:T(8,128)(2,1)} custom-call(s32[2]{0:T(128)} %pad_add_fusion.place, f32[128,3072]{1,0:T(8,128)} %shard_map.130.local, bf16[128,2048]{1,0:T(8,128)(2,1)} %get-tuple-element.28.c, f32[8,128,128]{2,1,0:T(8,128)} %get-tuple-element.25.cols, bf16[2,1536,128]{2,1,0:T(8,128)(2,1)} %get-tuple-element.37.mine, ...), custom_call_target="tpu_custom_call" | custom-call | tf_op jit(solution)/shard_map/pallas_call | solution.py:515
  (35 shorter events, 3.7 us)
Async XLA Ops:
  1.7 9.3 %collective-permute-start.2 = (f32[4,1804]{1,0:T(4,128)}, f32[4,1804]{1,0:T(4,128)S(1)}, u32[]{:S(2)}, u32[]{:S(2)}) collective-permute-start(f32[4,1804]{1,0:T(4,128)} %get-tuple-element.24), channel_id=1, source_target_pairs={{0,8},{1,9},{2,10},{3,11},{4,12},{5,13},{6,14},{7,15},{8,0},{9,1},... | collective-permute-start | bytes 86600 | tf_op jit(solution)/shard_map/ppermute | solution.py:322
  2.2 8.8 %collective-permute-start.3 = (f32[4,1804]{1,0:T(4,128)}, f32[4,1804]{1,0:T(4,128)S(1)}, u32[]{:S(2)}, u32[]{:S(2)}) collective-permute-start(f32[4,1804]{1,0:T(4,128)} %get-tuple-element.24), channel_id=1, source_target_pairs={{0,16},{1,17},{2,18},{3,19},{4,20},{5,21},{6,22},{7,23},{8,24},{9,... | collective-permute-start | bytes 86600 | tf_op jit(solution)/shard_map/ppermute | solution.py:322
  4.8 6.2 %collective-permute-start.4 = (f32[4,1804]{1,0:T(4,128)}, f32[4,1804]{1,0:T(4,128)S(1)}, u32[]{:S(2)}, u32[]{:S(2)}) collective-permute-start(f32[4,1804]{1,0:T(4,128)} %get-tuple-element.24), channel_id=1, source_target_pairs={{0,24},{1,25},{2,26},{3,27},{4,28},{5,29},{6,30},{7,31},{8,16},{9,... | collective-permute-start | bytes 86600 | tf_op jit(solution)/shard_map/ppermute | solution.py:322
  4.8 5.1 %collective-permute-start.1 = (bf16[1,7168]{1,0:T(2,128)(2,1)}, bf16[1,7168]{1,0:T(2,128)(2,1)S(1)}, u32[]{:S(2)}, u32[]{:S(2)}) collective-permute-start(bf16[1,7168]{1,0:T(2,128)(2,1)} %get-tuple-element.23), channel_id=1, source_target_pairs={{8,0},{16,8},{24,16},{1,24},{9,1},{17,9},{25,17},{2,25},{10,2},{18... | collective-permute-start | bytes 43016 | tf_op jit(solution)/shard_map/ppermute | solution.py:402
  6.1 4.1 %collective-permute-start = (bf16[2,7168]{1,0:T(2,128)(2,1)}, bf16[2,7168]{1,0:T(2,128)(2,1)S(1)}, u32[]{:S(2)}, u32[]{:S(2)}) collective-permute-start(bf16[2,7168]{1,0:T(2,128)(2,1)} %get-tuple-element.22), channel_id=1, source_target_pairs={{0,8},{8,16},{16,24},{24,1},{1,9},{9,17},{17,25},{25,2},{2,10},{10... | collective-permute-start | bytes 86024 | tf_op jit(solution)/shard_map/ppermute | solution.py:401
  16.1 12.5 %copy-start.5 = (f32[2,48,128]{2,1,0:T(8,128)S(1)}, f32[2,48,128]{2,1,0:T(8,128)}, u32[]{:S(2)}) copy-start(f32[2,48,128]{2,1,0:T(8,128)} %get-tuple-element.32) | copy-start | bytes 147460
  26.9 4.4 %collective-permute-start.5 = (bf16[2,1536,128]{2,1,0:T(8,128)(2,1)}, bf16[2,1536,128]{2,1,0:T(8,128)(2,1)S(1)}, u32[]{:S(2)}, u32[]{:S(2)}) collective-permute-start(bf16[2,1536,128]{2,1,0:T(8,128)(2,1)} %get-tuple-element.31), channel_id=1, source_target_pairs={{0,8},{1,9},{2,10},{3,11},{4,12},{5,13},{6,14},{7,15},{8,0},{9,1},... | collective-permute-start | bytes 2359304 | tf_op jit(solution)/shard_map/ppermute | solution.py:322
  28.5 2.2 %collective-permute-start.6 = (f32[2,48,128]{2,1,0:T(8,128)S(1)}, f32[2,48,128]{2,1,0:T(8,128)S(1)}, u32[]{:S(2)}, u32[]{:S(2)}) collective-permute-start(f32[2,48,128]{2,1,0:T(8,128)S(1)} %copy-done.5), channel_id=1, source_target_pairs={{0,8},{1,9},{2,10},{3,11},{4,12},{5,13},{6,14},{7,15},{8,0},{9,1},... | collective-permute-start | bytes 147464 | tf_op jit(solution)/shard_map/ppermute | solution.py:322
  31.3 0.9 copy-start
  34.9 15.1 %collective-permute-start.7 = (bf16[1536,128]{1,0:T(8,128)(2,1)}, bf16[1536,128]{1,0:T(8,128)(2,1)S(1)}, u32[]{:S(2)}, u32[]{:S(2)}) collective-permute-start(bf16[1536,128]{1,0:T(8,128)(2,1)} %get-tuple-element.33), channel_id=1, source_target_pairs={{0,16},{1,17},{2,18},{3,19},{4,20},{5,21},{6,22},{7,23},{8,24},{9,... | collective-permute-start | bytes 1179656 | tf_op jit(solution)/shard_map/ppermute | solution.py:322
  45.2 4.2 %collective-permute-start.8 = (f32[2,48,128]{2,1,0:T(8,128)S(1)}, f32[2,48,128]{2,1,0:T(8,128)S(1)}, u32[]{:S(2)}, u32[]{:S(2)}) collective-permute-start(f32[2,48,128]{2,1,0:T(8,128)S(1)} %add.17), channel_id=1, source_target_pairs={{0,16},{1,17},{2,18},{3,19},{4,20},{5,21},{6,22},{7,23},{8,24},{9,... | collective-permute-start | bytes 147464 | tf_op jit(solution)/shard_map/ppermute | solution.py:322
  50.0 0.8 copy-start.1
  89.8 8.5 %copy-start.2 = (bf16[8,192,128]{2,1,0:T(8,128)(2,1)}, bf16[8,192,128]{2,1,0:T(8,128)(2,1)S(1)}, u32[]{:S(2)}) copy-start(bf16[8,192,128]{2,1,0:T(8,128)(2,1)S(1)} %all_to_all.11) | copy-start | bytes 1179652
  89.8 12.9 %copy-start.6 = (bf16[3072]{0:T(1024)(128)(2,1)S(1)}, bf16[3072]{0:T(1024)(128)(2,1)}, u32[]{:S(2)}) copy-start(bf16[3072]{0:T(1024)(128)(2,1)} %param.25) | copy-start | bytes 18436
  89.8 8.5 %collective-permute-start.9 = (bf16[1536,128]{1,0:T(8,128)(2,1)S(1)}, bf16[1536,128]{1,0:T(8,128)(2,1)S(1)}, u32[]{:S(2)}, u32[]{:S(2)}) collective-permute-start(bf16[1536,128]{1,0:T(8,128)(2,1)S(1)} %bitcast.27), channel_id=1, source_target_pairs={{0,16},{1,17},{2,18},{3,19},{4,20},{5,21},{6,22},{7,23},{8,24},{9,... | collective-permute-start | bytes 1179656 | tf_op jit(solution)/shard_map/ppermute | solution.py:322
  98.3 0.8 copy-start.4
  102.7 2.5 %collective-permute-start.10 = (bf16[2,1536,128]{2,1,0:T(8,128)(2,1)}, bf16[2,1536,128]{2,1,0:T(8,128)(2,1)S(1)}, u32[]{:S(2)}, u32[]{:S(2)}) collective-permute-start(bf16[2,1536,128]{2,1,0:T(8,128)(2,1)} %get-tuple-element.38), channel_id=1, source_target_pairs={{0,8},{1,9},{2,10},{3,11},{4,12},{5,13},{6,14},{7,15},{8,0},{9,1},... | collective-permute-start | bytes 2359304 | tf_op jit(solution)/shard_map/ppermute | solution.py:322
  105.2 0.9 copy-start.3
